TPU v7x, 32 devices: a whole 2x2x4 slice. The times are simulated.
32 devices in a mesh: sp: 8 (over z, core), tp: 4 (over y, x).
Axes of the slice: x: 2, y: 2, z: 4, core: 2. Of those that a mesh axis runs over, the one named last changes fastest.
Arguments:
- moe_in: bfloat16 [1536, 2048], P('sp'), may hold values from -6 to 6
- cotangent: bfloat16 [1536, 2048], P('sp'), may hold values from -6 to 6
- routing: int32 [1536, 2], P('sp'), may hold values from 0 to 7, as said below
- route_weight: float32 [1536, 2], P('sp'), may hold values from 0.2 to 1
- w_gate: bfloat16 [8, 2048, 2048], P('sp', 'tp'), may hold values from -0.125 to 0.125
- w_up: bfloat16 [8, 2048, 2048], P('sp', 'tp'), may hold values from -0.125 to 0.125
- w_down: bfloat16 [8, 2048, 2048], P('sp', 'tp'), may hold values from -0.125 to 0.125
- gate_b: bfloat16 [1024, 1536], P('tp', 'sp'), may hold values from -6 to 6
- gate_c: bfloat16 [1024, 1536], P('tp', 'sp'), may hold values from -6 to 6
- value_x: bfloat16 [1024, 1536], P('tp', 'sp'), may hold values from -6 to 6
- conv_taps: float32 [3, 1024], P(None, 'tp'), may hold values from -3 to 3
- out_proj: bfloat16 [1024, 2048], P('tp'), may hold values from -0.1875 to 0.1875
Outputs:
- w_gate_grad: bfloat16 [8, 2048, 2048], P('sp', 'tp')
- w_up_grad: bfloat16 [8, 2048, 2048], P('sp', 'tp')
- w_down_grad: bfloat16 [8, 2048, 2048], P('sp', 'tp')
- moe_in_grad: bfloat16 [1536, 2048], P('sp', 'tp')
- proj_grad: float32 [1024, 2048], P('tp', 'sp')
- gate_b_grad: bfloat16 [1024, 1536], P('tp', 'sp')
- gate_c_grad: bfloat16 [1024, 1536], P('tp', 'sp')
- value_x_grad: bfloat16 [1024, 1536], P('tp', 'sp')
Inputs may be any that keep to these rules, and one draw needn't show every extreme that they name: `routing`: in each aligned block of 192 rows every expert is named exactly 48 times. The two entries of a row are different experts of one group; group g holds experts g * 2 to g * 2 + 1.
All inputs are finite; a program needn't handle non-finite values.
Results may differ from a plain program's by a relative error of at most 0.025.
Values may be sent and summed in bfloat16 or wider, within the bound.
A program may use at most 64 MiB of HBM per device.

v0:
```python
import jax
import jax.numpy as jnp
from jax import lax
from jax.experimental import pallas as pl
from jax.experimental.pallas import tpu as pltpu
from jax.sharding import PartitionSpec as P

TAPS = 3
GROUPS = 4
CORES = 2
MESH = pl.DeviceIdType.MESH


def place():
    s, t = lax.axis_index("sp"), lax.axis_index("tp")
    z, c = lax.div(s, CORES), lax.rem(s, CORES)
    x, y = lax.rem(t, 2), lax.div(t, 2)
    lanes = (t + 1 - 2 * x, t + 2 - 4 * y, 3 - t)
    return s, t, z, c, lanes


def greet(targets):
    barrier = pltpu.get_barrier_semaphore()
    for target in targets:
        pl.semaphore_signal(barrier, inc=1, device_id=target, device_id_type=MESH)
    pl.semaphore_wait(barrier, len(targets))


def span(index, width):
    return pl.ds(pl.multiple_of(index * width, width), width)


def remote(src, dst, send_sem, recv_sem, target):
    return pltpu.make_async_remote_copy(
        src_ref=src,
        dst_ref=dst,
        send_sem=send_sem,
        recv_sem=recv_sem,
        device_id=target,
        device_id_type=MESH,
    )


def half(quarter, side, width):
    return pl.ds(pl.multiple_of(quarter * width + side * (width // 2), width // 2), width // 2)


def dispatch_kernel(
    routing_ref,
    route_weight_ref,
    moe_ref,
    cot_ref,
    out_x,
    out_cot,
    rows,
    weights,
    landed,
    weight_in,
    s1,
    r1,
    s2,
    r2,
    s3,
    r3,
    s4,
    r4,
    sw,
    rw,
    sm,
    rm,
    own,
):
    s, t, z, c, lanes = place()
    tokens, model = moe_ref.shape
    cap = tokens // GROUPS
    width = model // 4
    mate = (CORES * z + 1 - c, t)
    ahead = [lax.rem(z + d, GROUPS) for d in range(GROUPS)]
    behind = [lax.rem(z + GROUPS - d, GROUPS) for d in range(GROUPS)]
    targets = (
        [(CORES * ahead[d] + c, t) for d in range(1, GROUPS)]
        + [(CORES * ahead[d] + 1 - c, t) for d in range(1, GROUPS)]
        + [(s, lanes[0]), (s, lanes[1]), mate]
    )
    barrier = pltpu.get_barrier_semaphore()
    for target in targets:
        pl.semaphore_signal(barrier, inc=1, device_id=target, device_id_type=MESH)
    down = lax.broadcasted_iota(jnp.int32, (tokens, tokens), 0)
    along = lax.broadcasted_iota(jnp.int32, (tokens, tokens), 1)
    lead = routing_ref[0:1, :]
    group = lax.div(lead, CORES).astype(jnp.float32)
    group_down = jnp.sum(jnp.where(down == along, group, 0.0), axis=1, keepdims=True)
    earlier = (group_down == group) & (down < along)
    rank = jnp.sum(jnp.where(earlier, 1.0, 0.0), axis=0, keepdims=True)
    select = group * cap + rank == down.astype(jnp.float32)
    is_even = lax.rem(lead, CORES) == 0
    by_core = [
        jnp.where(is_even, route_weight_ref[k : k + 1, :], route_weight_ref[1 - k : 2 - k, :])
        for k in range(CORES)
    ]
    permute = select.astype(jnp.float32).astype(jnp.bfloat16)
    rows[:, 0] = (
        jnp.dot(permute, moe_ref[...], preferred_element_type=jnp.float32)
        .astype(rows.dtype)
        .reshape(GROUPS, cap, model)
    )
    rows[:, 1] = (
        jnp.dot(permute, cot_ref[...], preferred_element_type=jnp.float32)
        .astype(rows.dtype)
        .reshape(GROUPS, cap, model)
    )
    columns = [
        jnp.sum(jnp.where(select, by_core[k], 0.0), axis=1, keepdims=True)
        for k in range(CORES)
    ]
    lane_at = lax.broadcasted_iota(jnp.int32, (tokens, 128), 1)
    weights[...] = jnp.where(lane_at == 0, columns[0], columns[1]).reshape(GROUPS, cap, 128)
    pl.semaphore_wait(barrier, len(targets))

    order = (2, 1, 3)
    mine = span(t, width)
    first = {}
    for d in order:
        first[d] = remote(
            rows.at[ahead[d], :, :, mine],
            landed.at[:, s, :, mine],
            s1.at[d - 1],
            r1.at[d - 1],
            (CORES * ahead[d] + c, t),
        )
        first[d].start()
    small = []
    for d in order:
        for k in range(2):
            core = c if k == 0 else 1 - c
            copy = remote(
                weights.at[ahead[d]],
                weight_in.at[s],
                sw.at[k, d - 1],
                rw.at[k, d - 1],
                (CORES * ahead[d] + core, t),
            )
            copy.start()
            small.append(copy)
    pair = [
        remote(rows.at[z], landed.at[:, s], sm.at[0], rm.at[0], mate),
        remote(weights.at[z], weight_in.at[s], sm.at[1], rm.at[1], mate),
    ]
    local = [
        pltpu.make_async_copy(rows.at[z], landed.at[:, s], own.at[0]),
        pltpu.make_async_copy(weights.at[z], weight_in.at[s], own.at[1]),
    ]
    for copy in pair + local:
        copy.start()

    def finish(source):
        at_core = lax.broadcasted_iota(jnp.int32, (cap, 128), 1) == c
        scale = jnp.sum(jnp.where(at_core, weight_in[source], 0.0), axis=1, keepdims=True)
        out_x[source] = landed[0, source]
        out_cot[source] = (scale * landed[1, source].astype(jnp.float32)).astype(out_cot.dtype)

    second = {}
    for d in order:
        first[d].wait_recv()
        block = landed.at[:, CORES * behind[d] + c, :, mine]
        for j in range(2):
            second[j, d] = remote(
                block, block, s2.at[j, d - 1], r2.at[j, d - 1], (s, lanes[j])
            )
            second[j, d].start()
    third = {}
    for d in order:
        for j in range(2):
            second[j, d].wait_recv()
        for j in range(2):
            block = landed.at[:, CORES * behind[d] + c, :, half(lanes[1 - j], j, width)]
            third[j, d] = remote(
                block, block, s3.at[j, d - 1], r3.at[j, d - 1], (s, lanes[j])
            )
            third[j, d].start()
    for copy in local:
        copy.wait()
    finish(s)
    for copy in pair:
        copy.wait()
    finish(CORES * z + 1 - c)
    for copy in small:
        copy.wait()
    fourth = {}
    for d in order:
        for j in range(2):
            third[j, d].wait_recv()
        block = landed.at[:, CORES * behind[d] + c]
        fourth[d] = remote(block, block, s4.at[d - 1], r4.at[d - 1], mate)
        fourth[d].start()
        finish(CORES * behind[d] + c)
    for d in order:
        fourth[d].wait_recv()
        finish(CORES * behind[d] + 1 - c)
    for group in (first, second, third, fourth):
        for copy in group.values():
            copy.wait_send()


def dispatch(routing, route_weight, moe_in, cotangent):
    tokens, model = moe_in.shape
    cap = tokens // GROUPS
    vmem = pl.BlockSpec(memory_space=pltpu.VMEM)
    dma = pltpu.SemaphoreType.DMA
    landing = jax.ShapeDtypeStruct((CORES * GROUPS, cap, model), moe_in.dtype)
    one, two = (GROUPS - 1,), (2, GROUPS - 1)
    return pl.pallas_call(
        dispatch_kernel,
        out_shape=(landing, landing),
        in_specs=[vmem] * 4,
        out_specs=(vmem, vmem),
        scratch_shapes=[
            pltpu.VMEM((GROUPS, 2, cap, model), moe_in.dtype),
            pltpu.VMEM((GROUPS, cap, 128), jnp.float32),
            pltpu.VMEM((2, CORES * GROUPS, cap, model), moe_in.dtype),
            pltpu.VMEM((CORES * GROUPS, cap, 128), jnp.float32),
        ]
        + [dma(one), dma(one)]
        + [dma(two) for _ in range(4)]
        + [dma(one), dma(one)]
        + [dma(two), dma(two)]
        + [dma((2,)) for _ in range(3)],
        compiler_params=pltpu.CompilerParams(collective_id=0, has_side_effects=True),
        name="dispatch",
    )(routing, route_weight, moe_in, cotangent)


def combine_kernel(part_ref, out_ref, mate_in, total, lane_in, done, sa, ra, sb, rb, sc, rc, sd, rd, se, re):
    s, t, z, c, lanes = place()
    width = part_ref.shape[-1] // 4
    mate = (CORES * z + 1 - c, t)
    ahead = [lax.rem(z + d, GROUPS) for d in range(GROUPS)]
    behind = [lax.rem(z + GROUPS - d, GROUPS) for d in range(GROUPS)]
    greet(
        [(CORES * ahead[d] + c, t) for d in range(1, GROUPS)]
        + [(s, lane) for lane in lanes]
        + [mate]
    )
    order = (2, 1, 3, 0)
    mine = span(t, width)
    swap = {}
    for d in order:
        swap[d] = remote(part_ref.at[ahead[d], 1 - c], mate_in.at[d], sa.at[d], ra.at[d], mate)
        swap[d].start()
    across = {}
    for d in order:
        swap[d].wait_recv()
        total[d] = (
            part_ref[ahead[d], c].astype(jnp.float32) + mate_in[d].astype(jnp.float32)
        ).astype(total.dtype)
        for j in (2, 0, 1):
            across[j, d] = remote(
                total.at[d, :, span(lanes[j], width)],
                lane_in.at[j, d],
                sb.at[j, d],
                rb.at[j, d],
                (s, lanes[j]),
            )
            across[j, d].start()
    home = {}
    for d in order:
        value = total[d, :, mine].astype(jnp.float32)
        for j in range(3):
            across[j, d].wait_recv()
            value = value + lane_in[j, d].astype(jnp.float32)
        value = value.astype(out_ref.dtype)
        if d == 0:
            out_ref[z, :, mine] = value
        else:
            done[d - 1] = value
            home[d] = remote(
                done.at[d - 1],
                out_ref.at[z, :, mine],
                sc.at[d - 1],
                rc.at[d - 1],
                (CORES * ahead[d] + c, t),
            )
            home[d].start()
    spread = {}
    for d in (0, 1, 3, 2):
        if d:
            home[d].wait_recv()
        block = out_ref.at[behind[d], :, mine]
        for j in range(2):
            spread[j, d] = remote(block, block, sd.at[j, d], rd.at[j, d], (s, lanes[j]))
            spread[j, d].start()
    relay = []
    for d in (0, 1, 3, 2):
        for j in range(2):
            spread[j, d].wait_recv()
        for j in range(2):
            block = out_ref.at[behind[d], :, half(lanes[1 - j], j, width)]
            copy = remote(block, block, se.at[j, d], re.at[j, d], (s, lanes[j]))
            copy.start()
            relay.append(copy)
    for copy in relay:
        copy.wait()
    for copy in spread.values():
        copy.wait_send()
    for copy in list(swap.values()) + list(across.values()) + list(home.values()):
        copy.wait_send()


def combine(part):
    groups, cores, cap, model = part.shape
    vmem = pl.BlockSpec(memory_space=pltpu.VMEM)
    dma = pltpu.SemaphoreType.DMA
    width = model // 4
    return pl.pallas_call(
        combine_kernel,
        out_shape=jax.ShapeDtypeStruct((groups, cap, model), part.dtype),
        in_specs=[vmem],
        out_specs=vmem,
        scratch_shapes=[
            pltpu.VMEM((groups, cap, model), part.dtype),
            pltpu.VMEM((groups, cap, model), part.dtype),
            pltpu.VMEM((3, groups, cap, width), part.dtype),
            pltpu.VMEM((groups - 1, cap, width), part.dtype),
            dma((groups,)),
            dma((groups,)),
            dma((3, groups)),
            dma((3, groups)),
            dma((groups - 1,)),
            dma((groups - 1,)),
            dma((2, groups)),
            dma((2, groups)),
            dma((2, groups)),
            dma((2, groups)),
        ],
        compiler_params=pltpu.CompilerParams(collective_id=1, has_side_effects=True),
        name="combine",
    )(part)


def project_kernel(part_ref, out_ref, far_in, mate_in, total, sa, ra, sb, rb):
    s, t, z, c, lanes = place()
    width = out_ref.shape[1]
    mate = (CORES * z + 1 - c, t)
    ahead = [lax.rem(z + d, GROUPS) for d in range(GROUPS)]
    greet([(CORES * ahead[d] + c, t) for d in range(1, GROUPS)] + [mate])
    order = (2, 1, 3, 0)
    swap = {}
    for d in order:
        cols = span(CORES * ahead[d] + 1 - c, width)
        swap[d] = remote(part_ref.at[:, cols], mate_in.at[d], sa.at[d], ra.at[d], mate)
        swap[d].start()
    far = {}
    for d in order:
        swap[d].wait_recv()
        cols = span(CORES * ahead[d] + c, width)
        value = part_ref[:, cols].astype(jnp.float32) + mate_in[d].astype(jnp.float32)
        if d == 0:
            out_ref[...] = value
        else:
            total[d - 1] = value.astype(total.dtype)
            far[d] = remote(
                total.at[d - 1],
                far_in.at[d - 1],
                sb.at[d - 1],
                rb.at[d - 1],
                (CORES * ahead[d] + c, t),
            )
            far[d].start()
    for d in range(1, GROUPS):
        far[d].wait_recv()
    for copy in list(swap.values()) + list(far.values()):
        copy.wait_send()


def project(part):
    channels, model = part.shape
    width = model // (CORES * GROUPS)
    vmem = pl.BlockSpec(memory_space=pltpu.VMEM)
    dma = pltpu.SemaphoreType.DMA
    return pl.pallas_call(
        project_kernel,
        out_shape=(
            jax.ShapeDtypeStruct((channels, width), jnp.float32),
            jax.ShapeDtypeStruct((GROUPS - 1, channels, width), part.dtype),
        ),
        in_specs=[vmem],
        out_specs=(vmem, vmem),
        scratch_shapes=[
            pltpu.VMEM((GROUPS, channels, width), part.dtype),
            pltpu.VMEM((GROUPS - 1, channels, width), part.dtype),
            dma((GROUPS,)),
            dma((GROUPS,)),
            dma((GROUPS - 1,)),
            dma((GROUPS - 1,)),
        ],
        compiler_params=pltpu.CompilerParams(collective_id=2, has_side_effects=True),
        name="project",
    )(part)


def from_behind(array, axis, by):
    count = lax.axis_size(axis)
    pairs = [(i, i + by) for i in range(count) if 0 <= i + by < count]
    return lax.ppermute(array, axis, pairs)


def on_device_general(
    moe_in,
    cotangent,
    routing,
    route_weight,
    w_gate,
    w_up,
    w_down,
    gate_b,
    gate_c,
    value_x,
    conv_taps,
    out_proj,
):
    tok_rows = routing.shape[0]
    top_routes = routing.shape[1]
    experts = lax.axis_size("sp")
    lane_count = lax.axis_size("tp")
    model_width = moe_in.shape[1]
    capacity = top_routes * tok_rows // experts
    flat_routes = routing.reshape(-1)
    route_count = flat_routes.shape[0]
    one_hot = (flat_routes[:, None] == jnp.arange(experts, dtype=jnp.int32)[None, :]).astype(
        jnp.int32
    )
    slot_rank = jnp.sum(jnp.cumsum(one_hot, axis=0) * one_hot, axis=1) - 1
    slot_index = flat_routes * capacity + slot_rank
    source = (
        jnp.zeros((route_count,), jnp.int32)
        .at[slot_index]
        .set(jnp.arange(route_count, dtype=jnp.int32))
    )
    owner_token = source // top_routes
    scales = route_weight.reshape(-1)[source][:, None]
    col_width = model_width // lane_count
    col_start = lax.axis_index("tp") * col_width
    rows_part = lax.dynamic_slice_in_dim(moe_in, col_start, col_width, 1)[owner_token]
    cot_slice = lax.dynamic_slice_in_dim(cotangent, col_start, col_width, 1)[owner_token]
    cot_part = (scales * cot_slice.astype(jnp.float32)).astype(jnp.bfloat16)
    moved = (
        lax.all_to_all(rows_part, "sp", split_axis=0, concat_axis=0, tiled=True),
        lax.all_to_all(cot_part, "sp", split_axis=0, concat_axis=0, tiled=True),
    )
    arrived, arrived_cot = (
        lax.all_gather(moved[0], "tp", axis=1, tiled=True),
        lax.all_gather(moved[1], "tp", axis=1, tiled=True),
    )
    contract_model = (((1,), (1,)), ((), ()))
    over_rows = (((0,), (0,)), ((), ()))
    gate_pre = lax.dot_general(
        arrived, w_gate[0], contract_model, preferred_element_type=jnp.float32
    )
    up_pre = lax.dot_general(arrived, w_up[0], contract_model, preferred_element_type=jnp.float32)
    sigmoid_gate = jax.nn.sigmoid(gate_pre)
    hidden = (gate_pre * sigmoid_gate * up_pre).astype(jnp.bfloat16)
    hidden_grad = lax.dot_general(
        arrived_cot, w_down[0], contract_model, preferred_element_type=jnp.float32
    )
    gate_grad = (
        hidden_grad * up_pre * sigmoid_gate * (1.0 + gate_pre * (1.0 - sigmoid_gate))
    ).astype(jnp.bfloat16)
    up_grad = (hidden_grad * gate_pre * sigmoid_gate).astype(jnp.bfloat16)
    w_gate_grad = lax.dot_general(
        gate_grad, arrived, over_rows, preferred_element_type=jnp.float32
    ).astype(jnp.bfloat16)[None]
    w_up_grad = lax.dot_general(
        up_grad, arrived, over_rows, preferred_element_type=jnp.float32
    ).astype(jnp.bfloat16)[None]
    w_down_grad = lax.dot_general(
        hidden, arrived_cot, over_rows, preferred_element_type=jnp.float32
    ).astype(jnp.bfloat16)[None]
    partial_value = jnp.dot(gate_grad, w_gate[0], preferred_element_type=jnp.float32) + jnp.dot(
        up_grad, w_up[0], preferred_element_type=jnp.float32
    )
    partial_value = lax.optimization_barrier(partial_value.astype(jnp.bfloat16)).astype(jnp.float32)
    summed = lax.psum_scatter(
        partial_value.astype(jnp.bfloat16), "tp", scatter_dimension=1, tiled=True
    )
    returned = lax.all_to_all(summed, "sp", split_axis=0, concat_axis=0, tiled=True)
    per_route = returned[slot_index].astype(jnp.float32)
    moe_in_grad = jnp.sum(per_route.reshape(tok_rows, top_routes, -1), axis=1).astype(jnp.bfloat16)
    full_grad = lax.all_gather(moe_in_grad, "tp", axis=1, tiled=True)
    stream_grad = (cotangent.astype(jnp.float32) + full_grad.astype(jnp.float32)).astype(
        jnp.bfloat16
    )
    mixed_in = lax.optimization_barrier(
        (gate_c.astype(jnp.float32) * value_x.astype(jnp.float32)).astype(jnp.bfloat16)
    )
    earlier = from_behind(mixed_in[:, tok_rows - (TAPS - 1) :], "sp", 1)
    extended = jnp.concatenate([earlier, mixed_in], axis=1).astype(jnp.float32)
    conv_out = jnp.zeros(mixed_in.shape, jnp.float32)
    for tap in range(TAPS):
        conv_out = conv_out + conv_taps[tap][:, None] * extended[:, tap : tap + tok_rows]
    mixer_act = (gate_b.astype(jnp.float32) * conv_out).astype(jnp.bfloat16)
    act_grad = lax.dot_general(
        out_proj, stream_grad, contract_model, preferred_element_type=jnp.float32
    )
    proj_rows = lax.psum_scatter(
        lax.dot_general(
            stream_grad, mixer_act, (((0,), (1,)), ((), ())), preferred_element_type=jnp.float32
        ).astype(jnp.bfloat16),
        "sp",
        scatter_dimension=0,
        tiled=True,
    ).astype(jnp.float32)
    proj_grad = proj_rows.T
    gate_b_grad = (act_grad * conv_out).astype(jnp.bfloat16)
    conv_grad = act_grad * gate_b.astype(jnp.float32)
    later = from_behind(conv_grad[:, : TAPS - 1], "sp", -1)
    extended_grad = jnp.concatenate([conv_grad, later], axis=1)
    mixed_grad = jnp.zeros(conv_grad.shape, jnp.float32)
    for tap in range(TAPS):
        offset = TAPS - 1 - tap
        mixed_grad = (
            mixed_grad + conv_taps[tap][:, None] * extended_grad[:, offset : offset + tok_rows]
        )
    gate_c_grad = (mixed_grad * value_x.astype(jnp.float32)).astype(jnp.bfloat16)
    value_x_grad = (mixed_grad * gate_c.astype(jnp.float32)).astype(jnp.bfloat16)
    return (
        w_gate_grad,
        w_up_grad,
        w_down_grad,
        moe_in_grad,
        proj_grad,
        gate_b_grad,
        gate_c_grad,
        value_x_grad,
    )


def on_device_paired(
    moe_in,
    cotangent,
    routing,
    route_weight,
    w_gate,
    w_up,
    w_down,
    gate_b,
    gate_c,
    value_x,
    conv_taps,
    out_proj,
):
    tok_rows = routing.shape[0]
    lane_count = lax.axis_size("tp")
    model_width = moe_in.shape[1]
    cap = tok_rows // GROUPS
    group = routing[:, 0] // CORES
    at = jnp.arange(tok_rows, dtype=jnp.int32)
    same = (group[:, None] == group[None, :]) & (at[:, None] < at[None, :])
    position = group * cap + jnp.sum(same.astype(jnp.int32), axis=0)
    select = position[None, :] == at[:, None]
    permute = select.astype(jnp.bfloat16)
    landed, landed_cot = dispatch(routing.T, route_weight.T, moe_in, cotangent)
    arrived = landed.reshape(-1, model_width)
    arrived_cot = landed_cot.reshape(-1, model_width)
    contract_model = (((1,), (1,)), ((), ()))
    over_rows = (((0,), (0,)), ((), ()))
    gate_pre = lax.dot_general(
        arrived, w_gate[0], contract_model, preferred_element_type=jnp.float32
    )
    up_pre = lax.dot_general(arrived, w_up[0], contract_model, preferred_element_type=jnp.float32)
    sigmoid_gate = jax.nn.sigmoid(gate_pre)
    hidden = (gate_pre * sigmoid_gate * up_pre).astype(jnp.bfloat16)
    hidden_grad = lax.dot_general(
        arrived_cot, w_down[0], contract_model, preferred_element_type=jnp.float32
    )
    gate_grad = (
        hidden_grad * up_pre * sigmoid_gate * (1.0 + gate_pre * (1.0 - sigmoid_gate))
    ).astype(jnp.bfloat16)
    up_grad = (hidden_grad * gate_pre * sigmoid_gate).astype(jnp.bfloat16)
    w_gate_grad = lax.dot_general(
        gate_grad, arrived, over_rows, preferred_element_type=jnp.float32
    ).astype(jnp.bfloat16)[None]
    w_up_grad = lax.dot_general(
        up_grad, arrived, over_rows, preferred_element_type=jnp.float32
    ).astype(jnp.bfloat16)[None]
    w_down_grad = lax.dot_general(
        hidden, arrived_cot, over_rows, preferred_element_type=jnp.float32
    ).astype(jnp.bfloat16)[None]
    partial_value = jnp.dot(gate_grad, w_gate[0], preferred_element_type=jnp.float32) + jnp.dot(
        up_grad, w_up[0], preferred_element_type=jnp.float32
    )
    summed = combine(
        partial_value.astype(jnp.bfloat16).reshape(GROUPS, CORES, cap, model_width)
    )
    full_grad = lax.dot_general(
        permute,
        summed.reshape(tok_rows, model_width),
        over_rows,
        preferred_element_type=jnp.float32,
    ).astype(jnp.bfloat16)
    col_width = model_width // lane_count
    moe_in_grad = lax.dynamic_slice_in_dim(
        full_grad, lax.axis_index("tp") * col_width, col_width, 1
    )
    stream_grad = (cotangent.astype(jnp.float32) + full_grad.astype(jnp.float32)).astype(
        jnp.bfloat16
    )
    mixed_in = lax.optimization_barrier(
        (gate_c.astype(jnp.float32) * value_x.astype(jnp.float32)).astype(jnp.bfloat16)
    )
    earlier = from_behind(mixed_in[:, tok_rows - (TAPS - 1) :], "sp", 1)
    extended = jnp.concatenate([earlier, mixed_in], axis=1).astype(jnp.float32)
    conv_out = jnp.zeros(mixed_in.shape, jnp.float32)
    for tap in range(TAPS):
        conv_out = conv_out + conv_taps[tap][:, None] * extended[:, tap : tap + tok_rows]
    mixer_act = (gate_b.astype(jnp.float32) * conv_out).astype(jnp.bfloat16)
    act_grad = lax.dot_general(
        out_proj, stream_grad, contract_model, preferred_element_type=jnp.float32
    )
    near, far = project(
        jnp.dot(mixer_act, stream_grad, preferred_element_type=jnp.float32).astype(jnp.bfloat16)
    )
    proj_grad = near + (far[0].astype(jnp.float32) + far[1].astype(jnp.float32)) + far[2].astype(jnp.float32)
    gate_b_grad = (act_grad * conv_out).astype(jnp.bfloat16)
    conv_grad = act_grad * gate_b.astype(jnp.float32)
    later = from_behind(conv_grad[:, : TAPS - 1], "sp", -1)
    extended_grad = jnp.concatenate([conv_grad, later], axis=1)
    mixed_grad = jnp.zeros(conv_grad.shape, jnp.float32)
    for tap in range(TAPS):
        offset = TAPS - 1 - tap
        mixed_grad = (
            mixed_grad + conv_taps[tap][:, None] * extended_grad[:, offset : offset + tok_rows]
        )
    gate_c_grad = (mixed_grad * value_x.astype(jnp.float32)).astype(jnp.bfloat16)
    value_x_grad = (mixed_grad * gate_c.astype(jnp.float32)).astype(jnp.bfloat16)
    return (
        w_gate_grad,
        w_up_grad,
        w_down_grad,
        moe_in_grad,
        proj_grad,
        gate_b_grad,
        gate_c_grad,
        value_x_grad,
    )


def on_device(*args):
    routes = args[2].shape[1]
    experts, lane_count = lax.axis_size("sp"), lax.axis_size("tp")
    if experts == CORES * GROUPS and routes == CORES and lane_count == 4:
        return on_device_paired(*args)
    return on_device_general(*args)


def solution(mesh):
    in_specs = (
        P("sp", None),
        P("sp", None),
        P("sp", None),
        P("sp", None),
        P("sp", "tp", None),
        P("sp", "tp", None),
        P("sp", "tp", None),
        P("tp", "sp"),
        P("tp", "sp"),
        P("tp", "sp"),
        P(None, "tp"),
        P("tp", None),
    )
    out_specs = (
        P("sp", "tp", None),
        P("sp", "tp", None),
        P("sp", "tp", None),
        P("sp", "tp"),
        P("tp", "sp"),
        P("tp", "sp"),
        P("tp", "sp"),
        P("tp", "sp"),
    )
    return jax.shard_map(
        on_device, mesh=mesh, in_specs=in_specs, out_specs=out_specs, check_vma=False
    )
```

profile of v0, /device:TPU:0, one launch (start us, length us, event | category | flops | bytes accessed | tf_op | source)
XLA Modules:
  0.0 106.9 jit_solution(5532479350543000002)
XLA Ops:
  0.6 0.0 copy-start
  0.6 1.1 %fusion.19 = bf16[256,192]{0,1:T(8,128)(2,1)S(1)} fusion(bf16[256,192]{0,1:T(8,128)(2,1)} %param.21, bf16[256,192]{0,1:T(8,128)(2,1)} %param.20), kind=kLoop, calls=%fused_computation.40 | loop fusion | flops 196608 | bytes 294912 | tf_op jit(solution)/shard_map/convert_element_type | solution.py:608
  1.8 2.4 %collective-permute-start = (bf16[256,2]{0,1:T(2,128)(2,1)S(1)}, bf16[256,2]{0,1:T(2,128)(2,1)S(1)}, u32[]{:S(2)}, u32[]{:S(2)}) collective-permute-start(bf16[256,2]{0,1:T(2,128)(2,1)S(1)} %slice.59), channel_id=1, source_target_pairs={{0,4},{4,8},{8,12},{12,16},{16,20},{20,24},{24,28},{1,5},{5,9},{9,... | collective-permute-start | bytes 3080 | tf_op jit(solution)/shard_map/ppermute | solution.py:404
  4.2 0.7 and_select_fusion
  4.9 31.2 %dispatch.1 = (bf16[8,48,2048]{2,1,0:T(8,128)(2,1)}, bf16[8,48,2048]{2,1,0:T(8,128)(2,1)}) custom-call(s32[2,192]{1,0:T(2,128)} %bitcast.63, f32[2,192]{1,0:T(2,128)} %bitcast.65, bf16[192,2048]{1,0:T(8,128)(2,1)} %moe_ref.1, bf16[192,2048]{1,0:T(8,128)(2,1)} %cot_ref.1), custom_call_target="tpu_custom_call" | custom-call | tf_op jit(solution)/shard_map/dispatch/pallas_call | solution.py:212
  36.1 0.0 copy-start.2
  36.1 2.6 %fusion.5 = f32[384,512]{1,0:T(8,128)S(1)} fusion(bf16[384,2048]{1,0:T(8,128)(2,1)} %bitcast.66, bf16[1,512,2048]{2,1,0:T(8,128)(2,1)S(1)} %copy-done), kind=kOutput, calls=%fused_computation.11 | convolution fusion | flops 805306368 | bytes 4456448 | tf_op jit(solution)/shard_map/dot_general | solution.py:566
  38.7 0.0 copy-start.7
  38.7 1.0 fusion.8
  39.7 0.6 copy-done.7
  40.3 0.4 copy-done.9
  40.7 1.2 %multiply_convert_fusion.1 = (bf16[384,512]{1,0:T(8,128)(2,1)S(1)}, bf16[384,512]{1,0:T(8,128)(2,1)S(1)}) fusion(f32[384,512]{1,0:T(8,128)S(1)} %fusion.5, f32[384,512]{1,0:T(8,128)S(1)} %fusion.8, bf16[384,2048]{1,0:T(8,128)(2,1)S(1)} %bitcast.70, bf16[1,512,2048]{2,1,0:T(8,128)(2,1)S(1)} %copy-done.7), kind=kOutput, calls=%fused_computation.21 | convolution fusion | flops 807862272 | bytes 6029312 | tf_op jit(solution)/shard_map/dot_general | solution.py:572
  42.0 1.0 fusion.3
  42.9 2.6 %fusion = bf16[1,512,2048]{2,1,0:T(8,128)(2,1)} fusion(bf16[384,512]{1,0:T(8,128)(2,1)S(1)} %get-tuple-element.21, bf16[384,2048]{1,0:T(8,128)(2,1)S(1)} %bitcast.68), kind=kOutput, calls=%fused_computation.4 | convolution fusion | flops 806354944 | bytes 4063232 | tf_op jit(solution)/shard_map/dot_general | solution.py:579
  45.5 2.7 %fusion.2 = bf16[1,512,2048]{2,1,0:T(8,128)(2,1)} fusion(bf16[384,2048]{1,0:T(8,128)(2,1)S(1)} %bitcast.71, f32[384,512]{1,0:T(8,128)S(1)} %fusion.8, f32[384,512]{1,0:T(8,128)S(1)} %fusion.5), kind=kOutput, calls=%fused_computation.6 | convolution fusion | flops 807534592 | bytes 5242880 | tf_op jit(solution)/shard_map/dot_general | solution.py:585
  48.2 2.6 %fusion.1 = bf16[1,512,2048]{2,1,0:T(8,128)(2,1)} fusion(bf16[384,512]{1,0:T(8,128)(2,1)S(1)} %get-tuple-element.20, bf16[384,2048]{1,0:T(8,128)(2,1)S(1)} %bitcast.69), kind=kOutput, calls=%fused_computation.5 | convolution fusion | flops 806354944 | bytes 4063232 | tf_op jit(solution)/shard_map/dot_general | solution.py:582
  50.8 2.2 %add_convert_fusion = bf16[384,2048]{1,0:T(8,128)(2,1)} fusion(f32[384,2048]{1,0:T(8,128)S(1)} %fusion.3, bf16[384,512]{1,0:T(8,128)(2,1)S(1)} %get-tuple-element.20, bf16[1,512,2048]{2,1,0:T(8,128)(2,1)S(1)} %copy-done.2), kind=kOutput, calls=%fused_computation | convolution fusion | flops 806879232 | bytes 7208960 | tf_op jit(solution)/shard_map/dot_general | solution.py:588
  53.0 25.9 %combine.1 = bf16[4,48,2048]{2,1,0:T(8,128)(2,1)} custom-call(bf16[4,2,48,2048]{3,2,1,0:T(8,128)(2,1)} %bitcast.53), custom_call_target="tpu_custom_call" | custom-call | tf_op jit(solution)/shard_map/combine/pallas_call | solution.py:314
  79.0 0.1 convert_reduce_fusion
  79.1 1.6 %convolution_convert_fusion.4 = bf16[192,2048]{1,0:T(8,128)(2,1)S(1)} fusion(bf16[192,2048]{1,0:T(8,128)(2,1)} %bitcast.54, s32[192]{0:T(256)S(1)} %multiply_add_fusion), kind=kOutput, calls=%fused_computation.8 | convolution fusion | flops 151425024 | bytes 1573632 | tf_op jit(solution)/shard_map/dot_general | solution.py:594
  80.7 0.0 copy-start.1
  80.7 0.7 constant_dynamic-slice_fusion
  81.4 2.6 %multiply_convert_fusion.4 = (bf16[256,192]{0,1:T(8,128)(2,1)}, f32[256,192]{0,1:T(8,128)S(1)}, f32[256,192]{0,1:T(8,128)S(1)}) fusion(f32[256,194]{0,1:T(8,128)S(1)} %maximum_convert_fusion, f32[256]{0:T(256)S(1)} %bitcast.57, f32[256]{0:T(256)S(1)} %bitcast.59, f32[256]{0:T(256)S(1)} %bitcast.55, bf16[256,192]{0,1:T(8,128)(2,1)S(1)} %copy-done.3, ...), kind=kOutput, calls=%fused_computation.49 | convolution fusion | flops 203341824 | bytes 3804160 | tf_op jit(solution)/shard_map/dot_general | solution.py:616
  84.1 1.3 %collective-permute-start.1 = (f32[256,2]{0,1:T(2,128)S(1)}, f32[256,2]{0,1:T(2,128)S(1)}, u32[]{:S(2)}, u32[]{:S(2)}) collective-permute-start(f32[256,2]{0,1:T(2,128)S(1)} %slice.63), channel_id=1, source_target_pairs={{4,0},{8,4},{12,8},{16,12},{20,16},{24,20},{28,24},{5,1},{9,5},{13... | collective-permute-start | bytes 6152 | tf_op jit(solution)/shard_map/ppermute | solution.py:404
  85.4 0.0 copy-start.4
  85.4 0.0 copy-start.5
  85.4 1.5 %convolution_convert_fusion.3.part_ref = bf16[256,2048]{1,0:T(8,128)(2,1)} fusion(bf16[192,2048]{1,0:T(8,128)(2,1)S(1)} %convolution_convert_fusion.4, bf16[192,2048]{1,0:T(8,128)(2,1)S(1)} %copy-done.1, f32[256,192]{0,1:T(8,128)S(1)} %get-tuple-element.19, bf16[256,192]{0,1:T(8,128)(2,1)S(1)} %copy-done.3), kind=kOutput, calls=%fused_computation.7 | convolution fusion | flops 203571200 | bytes 2916352 | tf_op jit(solution)/shard_map/dot_general | solution.py:620
  86.9 16.8 %project.1 = (f32[256,256]{1,0:T(8,128)}, bf16[3,256,256]{2,1,0:T(8,128)(2,1)}) custom-call(bf16[256,2048]{1,0:T(8,128)(2,1)} %convolution_convert_fusion.3.part_ref), custom_call_target="tpu_custom_call" | custom-call | tf_op jit(solution)/shard_map/project/pallas_call | solution.py:380
  103.7 1.9 %convert_add_fusion = f32[256,256]{1,0:T(8,128)} fusion(f32[256,256]{1,0:T(8,128)} %get-tuple-element.14, bf16[3,256,256]{2,1,0:T(8,128)(2,1)} %get-tuple-element.15), kind=kLoop, calls=%fused_computation.25 | loop fusion | flops 393216 | bytes 917504 | tf_op jit(solution)/shard_map/add | solution.py:622
  105.5 0.0 collective-permute-done.1
  105.6 0.7 fusion.18
  106.3 0.7 fusion.20
  (19 shorter events, 0.1 us)
Async XLA Ops:
  0.6 35.4 %copy-start = (bf16[1,512,2048]{2,1,0:T(8,128)(2,1)S(1)}, bf16[1,512,2048]{2,1,0:T(8,128)(2,1)}, u32[]{:S(2)}) copy-start(bf16[1,512,2048]{2,1,0:T(8,128)(2,1)} %param.16) | copy-start | bytes 6291460
  1.8 79.6 %collective-permute-start = (bf16[256,2]{0,1:T(2,128)(2,1)S(1)}, bf16[256,2]{0,1:T(2,128)(2,1)S(1)}, u32[]{:S(2)}, u32[]{:S(2)}) collective-permute-start(bf16[256,2]{0,1:T(2,128)(2,1)S(1)} %slice.59), channel_id=1, source_target_pairs={{0,4},{4,8},{8,12},{12,16},{16,20},{20,24},{24,28},{1,5},{5,9},{9,... | collective-permute-start | bytes 3080 | tf_op jit(solution)/shard_map/ppermute | solution.py:404
  36.1 2.6 %copy-start.2 = (bf16[1,512,2048]{2,1,0:T(8,128)(2,1)S(1)}, bf16[1,512,2048]{2,1,0:T(8,128)(2,1)}, u32[]{:S(2)}) copy-start(bf16[1,512,2048]{2,1,0:T(8,128)(2,1)} %param.17) | copy-start | bytes 6291460
  36.1 2.6 %copy-start.8 = (bf16[8,48,2048]{2,1,0:T(8,128)(2,1)S(1)}, bf16[8,48,2048]{2,1,0:T(8,128)(2,1)}, u32[]{:S(2)}) copy-start(bf16[8,48,2048]{2,1,0:T(8,128)(2,1)} %get-tuple-element.13) | copy-start | bytes 4718596
  38.7 1.6 %copy-start.7 = (bf16[1,512,2048]{2,1,0:T(8,128)(2,1)S(1)}, bf16[1,512,2048]{2,1,0:T(8,128)(2,1)}, u32[]{:S(2)}) copy-start(bf16[1,512,2048]{2,1,0:T(8,128)(2,1)} %param.18) | copy-start | bytes 6291460
  38.7 2.0 %copy-start.9 = (bf16[8,48,2048]{2,1,0:T(8,128)(2,1)S(1)}, bf16[8,48,2048]{2,1,0:T(8,128)(2,1)}, u32[]{:S(2)}) copy-start(bf16[8,48,2048]{2,1,0:T(8,128)(2,1)} %get-tuple-element.12) | copy-start | bytes 4718596
  53.0 26.1 %copy-start.6 = (f32[3,256]{1,0:T(4,128)S(1)}, f32[3,256]{1,0:T(4,128)}, u32[]{:S(2)}) copy-start(f32[3,256]{1,0:T(4,128)} %param.22) | copy-start | bytes 9220
  53.0 28.4 %copy-start.3 = (bf16[256,192]{0,1:T(8,128)(2,1)S(1)}, bf16[256,192]{0,1:T(8,128)(2,1)}, u32[]{:S(2)}) copy-start(bf16[256,192]{0,1:T(8,128)(2,1)} %param.19) | copy-start | bytes 294916
  80.7 4.7 %copy-start.1 = (bf16[192,2048]{1,0:T(8,128)(2,1)S(1)}, bf16[192,2048]{1,0:T(8,128)(2,1)}, u32[]{:S(2)}) copy-start(bf16[192,2048]{1,0:T(8,128)(2,1)} %cot_ref.1) | copy-start | bytes 2359300
  84.1 21.5 %collective-permute-start.1 = (f32[256,2]{0,1:T(2,128)S(1)}, f32[256,2]{0,1:T(2,128)S(1)}, u32[]{:S(2)}, u32[]{:S(2)}) collective-permute-start(f32[256,2]{0,1:T(2,128)S(1)} %slice.63), channel_id=1, source_target_pairs={{4,0},{8,4},{12,8},{16,12},{20,16},{24,20},{28,24},{5,1},{9,5},{13... | collective-permute-start | bytes 6152 | tf_op jit(solution)/shard_map/ppermute | solution.py:404
  85.4 20.2 %copy-start.4 = (bf16[256,192]{0,1:T(8,128)(2,1)S(1)}, bf16[256,192]{0,1:T(8,128)(2,1)}, u32[]{:S(2)}) copy-start(bf16[256,192]{0,1:T(8,128)(2,1)} %param.20) | copy-start | bytes 294916
  85.4 20.9 %copy-start.5 = (bf16[256,192]{0,1:T(8,128)(2,1)S(1)}, bf16[256,192]{0,1:T(8,128)(2,1)}, u32[]{:S(2)}) copy-start(bf16[256,192]{0,1:T(8,128)(2,1)} %param.21) | copy-start | bytes 294916
where the time goes:
time: 107 us
  Pallas kernels  73.9 us (69%)
  matrix products  21.5 us (20%)
  other arithmetic  5.23 us (5%)
  starting transfers between devices  3.68 us (3%)
  local copies, waits for them, and re-layouts  1.77 us (2%)
    pallas_call x1, Pallas kernels, dispatch(): pl.pallas_call(dispatch_kernel, out_shape=(landing, landing), in_specs=[v...  31.2 us
    pallas_call x1, Pallas kernels, combine(): pl.pallas_call(combine_kernel, out_shape=jax.ShapeDtypeStruct((groups, ca...  25.9 us
    pallas_call x1, Pallas kernels, project(): pl.pallas_call(project_kernel, out_shape=(jax.ShapeDtypeStruct((channels,...  16.8 us
    ppermute x2, starting transfers between devices, from_behind(): return lax.ppermute(array, axis, pairs)  3.68 us
    dot_general x1, matrix products, on_device_paired(): lax.dot_general(hidden, arrived_cot, over_rows, preferred_element_type=jn...  2.67 us
    dot_general x1, matrix products, on_device_paired(): lax.dot_general(out_proj, stream_grad, contract_model, preferred_element_...  2.64 us
    dot_general x1, matrix products, on_device_paired(): lax.dot_general(gate_grad, arrived, over_rows, preferred_element_type=jnp...  2.61 us
    dot_general x1, matrix products, on_device_paired(): lax.dot_general(up_grad, arrived, over_rows, preferred_element_type=jnp.f...  2.61 us
  transfers between devices with their start and end apart: 2, of which 0 were waited for; matrix products, arithmetic and copies ran while one was open for 21% of the time, Pallas kernels for 69%

commit v1 on v0

v1 whole, which is shorter than its diff:
```python
import functools
import types

import jax
import jax.numpy as jnp
from jax import lax
from jax.experimental import pallas as pl
from jax.experimental.pallas import tpu as pltpu
from jax.sharding import PartitionSpec as P

TAPS = 3
GROUPS = 4
CORES = 2
MESH = pl.DeviceIdType.MESH


def place():
    s, t = lax.axis_index("sp"), lax.axis_index("tp")
    z, c = lax.div(s, CORES), lax.rem(s, CORES)
    x, y = lax.rem(t, 2), lax.div(t, 2)
    lanes = (t + 1 - 2 * x, t + 2 - 4 * y, 3 - t)
    return s, t, z, c, lanes


def span(index, width):
    return pl.ds(pl.multiple_of(index * width, width), width)


def remote(src, dst, send_sem, recv_sem, target):
    return pltpu.make_async_remote_copy(
        src_ref=src,
        dst_ref=dst,
        send_sem=send_sem,
        recv_sem=recv_sem,
        device_id=target,
        device_id_type=MESH,
    )


def half(quarter, side, width):
    return pl.ds(pl.multiple_of(quarter * width + side * (width // 2), width // 2), width // 2)


def from_behind(array, axis, by):
    count = lax.axis_size(axis)
    pairs = [(i, i + by) for i in range(count) if 0 <= i + by < count]
    return lax.ppermute(array, axis, pairs)


def on_device_general(
    moe_in,
    cotangent,
    routing,
    route_weight,
    w_gate,
    w_up,
    w_down,
    gate_b,
    gate_c,
    value_x,
    conv_taps,
    out_proj,
):
    tok_rows = routing.shape[0]
    top_routes = routing.shape[1]
    experts = lax.axis_size("sp")
    lane_count = lax.axis_size("tp")
    model_width = moe_in.shape[1]
    capacity = top_routes * tok_rows // experts
    flat_routes = routing.reshape(-1)
    route_count = flat_routes.shape[0]
    one_hot = (flat_routes[:, None] == jnp.arange(experts, dtype=jnp.int32)[None, :]).astype(
        jnp.int32
    )
    slot_rank = jnp.sum(jnp.cumsum(one_hot, axis=0) * one_hot, axis=1) - 1
    slot_index = flat_routes * capacity + slot_rank
    source = (
        jnp.zeros((route_count,), jnp.int32)
        .at[slot_index]
        .set(jnp.arange(route_count, dtype=jnp.int32))
    )
    owner_token = source // top_routes
    scales = route_weight.reshape(-1)[source][:, None]
    col_width = model_width // lane_count
    col_start = lax.axis_index("tp") * col_width
    rows_part = lax.dynamic_slice_in_dim(moe_in, col_start, col_width, 1)[owner_token]
    cot_slice = lax.dynamic_slice_in_dim(cotangent, col_start, col_width, 1)[owner_token]
    cot_part = (scales * cot_slice.astype(jnp.float32)).astype(jnp.bfloat16)
    moved = (
        lax.all_to_all(rows_part, "sp", split_axis=0, concat_axis=0, tiled=True),
        lax.all_to_all(cot_part, "sp", split_axis=0, concat_axis=0, tiled=True),
    )
    arrived, arrived_cot = (
        lax.all_gather(moved[0], "tp", axis=1, tiled=True),
        lax.all_gather(moved[1], "tp", axis=1, tiled=True),
    )
    contract_model = (((1,), (1,)), ((), ()))
    over_rows = (((0,), (0,)), ((), ()))
    gate_pre = lax.dot_general(
        arrived, w_gate[0], contract_model, preferred_element_type=jnp.float32
    )
    up_pre = lax.dot_general(arrived, w_up[0], contract_model, preferred_element_type=jnp.float32)
    sigmoid_gate = jax.nn.sigmoid(gate_pre)
    hidden = (gate_pre * sigmoid_gate * up_pre).astype(jnp.bfloat16)
    hidden_grad = lax.dot_general(
        arrived_cot, w_down[0], contract_model, preferred_element_type=jnp.float32
    )
    gate_grad = (
        hidden_grad * up_pre * sigmoid_gate * (1.0 + gate_pre * (1.0 - sigmoid_gate))
    ).astype(jnp.bfloat16)
    up_grad = (hidden_grad * gate_pre * sigmoid_gate).astype(jnp.bfloat16)
    w_gate_grad = lax.dot_general(
        gate_grad, arrived, over_rows, preferred_element_type=jnp.float32
    ).astype(jnp.bfloat16)[None]
    w_up_grad = lax.dot_general(
        up_grad, arrived, over_rows, preferred_element_type=jnp.float32
    ).astype(jnp.bfloat16)[None]
    w_down_grad = lax.dot_general(
        hidden, arrived_cot, over_rows, preferred_element_type=jnp.float32
    ).astype(jnp.bfloat16)[None]
    partial_value = jnp.dot(gate_grad, w_gate[0], preferred_element_type=jnp.float32) + jnp.dot(
        up_grad, w_up[0], preferred_element_type=jnp.float32
    )
    partial_value = lax.optimization_barrier(partial_value.astype(jnp.bfloat16)).astype(jnp.float32)
    summed = lax.psum_scatter(
        partial_value.astype(jnp.bfloat16), "tp", scatter_dimension=1, tiled=True
    )
    returned = lax.all_to_all(summed, "sp", split_axis=0, concat_axis=0, tiled=True)
    per_route = returned[slot_index].astype(jnp.float32)
    moe_in_grad = jnp.sum(per_route.reshape(tok_rows, top_routes, -1), axis=1).astype(jnp.bfloat16)
    full_grad = lax.all_gather(moe_in_grad, "tp", axis=1, tiled=True)
    stream_grad = (cotangent.astype(jnp.float32) + full_grad.astype(jnp.float32)).astype(
        jnp.bfloat16
    )
    mixed_in = lax.optimization_barrier(
        (gate_c.astype(jnp.float32) * value_x.astype(jnp.float32)).astype(jnp.bfloat16)
    )
    earlier = from_behind(mixed_in[:, tok_rows - (TAPS - 1) :], "sp", 1)
    extended = jnp.concatenate([earlier, mixed_in], axis=1).astype(jnp.float32)
    conv_out = jnp.zeros(mixed_in.shape, jnp.float32)
    for tap in range(TAPS):
        conv_out = conv_out + conv_taps[tap][:, None] * extended[:, tap : tap + tok_rows]
    mixer_act = (gate_b.astype(jnp.float32) * conv_out).astype(jnp.bfloat16)
    act_grad = lax.dot_general(
        out_proj, stream_grad, contract_model, preferred_element_type=jnp.float32
    )
    proj_rows = lax.psum_scatter(
        lax.dot_general(
            stream_grad, mixer_act, (((0,), (1,)), ((), ())), preferred_element_type=jnp.float32
        ).astype(jnp.bfloat16),
        "sp",
        scatter_dimension=0,
        tiled=True,
    ).astype(jnp.float32)
    proj_grad = proj_rows.T
    gate_b_grad = (act_grad * conv_out).astype(jnp.bfloat16)
    conv_grad = act_grad * gate_b.astype(jnp.float32)
    later = from_behind(conv_grad[:, : TAPS - 1], "sp", -1)
    extended_grad = jnp.concatenate([conv_grad, later], axis=1)
    mixed_grad = jnp.zeros(conv_grad.shape, jnp.float32)
    for tap in range(TAPS):
        offset = TAPS - 1 - tap
        mixed_grad = (
            mixed_grad + conv_taps[tap][:, None] * extended_grad[:, offset : offset + tok_rows]
        )
    gate_c_grad = (mixed_grad * value_x.astype(jnp.float32)).astype(jnp.bfloat16)
    value_x_grad = (mixed_grad * gate_c.astype(jnp.float32)).astype(jnp.bfloat16)
    return (
        w_gate_grad,
        w_up_grad,
        w_down_grad,
        moe_in_grad,
        proj_grad,
        gate_b_grad,
        gate_c_grad,
        value_x_grad,
    )


def last_dims(lhs, rhs):
    return lax.dot_general(lhs, rhs, (((1,), (1,)), ((), ())), preferred_element_type=jnp.float32)


def first_dims(lhs, rhs):
    return lax.dot_general(lhs, rhs, (((0,), (0,)), ((), ())), preferred_element_type=jnp.float32)


def plain(lhs, rhs):
    return jnp.dot(lhs, rhs, preferred_element_type=jnp.float32)


def step_kernel(names, *refs):
    r = types.SimpleNamespace(**dict(zip(names, refs)))
    s, t, z, c, lanes = place()
    tokens, model = r.moe.shape
    chan = r.gate_b.shape[1]
    cap = tokens // GROUPS
    width = model // 4
    hid_rows = r.w_gate.shape[0]
    devices = CORES * GROUPS
    f32, b16 = jnp.float32, jnp.bfloat16
    far = [z, z + 1 - 2 * lax.rem(z, 2), z + 2 - 4 * lax.div(z, 2), 3 - z]
    peer = [(CORES * far[d] + c, t) for d in range(GROUPS)]
    mate = (CORES * z + 1 - c, t)
    after, before = (lax.rem(s + 1, devices), t), (lax.rem(s + devices - 1, devices), t)
    side_z = lax.rem(z + GROUPS + 2 * c - 1, GROUPS)
    side = (CORES * side_z + 1 - c, t)
    lane = [(s, lanes[j]) for j in range(3)]
    mine = span(t, width)

    loads = {}
    order = ("moe", "cot", "gate_c", "value_x", "w_gate", "w_up", "w_down", "gate_b", "taps", "out_proj")
    for i, key in enumerate(order):
        loads[key] = pltpu.make_async_copy(getattr(r, key), getattr(r, "v_" + key), r.load.at[i])
        loads[key].start()
    targets = peer[1:] + [mate] + lane + [side]
    barrier = pltpu.get_barrier_semaphore()
    for target in targets:
        pl.semaphore_signal(barrier, inc=1, device_id=target, device_id_type=MESH)

    down = lax.broadcasted_iota(jnp.int32, (tokens, tokens), 0)
    along = lax.broadcasted_iota(jnp.int32, (tokens, tokens), 1)
    eye = down == along

    def column(row):
        return jnp.sum(jnp.where(eye, row, 0.0), axis=1, keepdims=True)

    lead = r.routing[0:1, :]
    group = lax.div(lead, CORES)
    low, high = lax.rem(group, 2), lax.div(group, 2)
    z_low, z_high = lax.rem(z, 2), lax.div(z, 2)
    slot = (low + z_low - 2 * low * z_low) + 2 * (high + z_high - 2 * high * z_high)
    slot = slot.astype(f32)
    earlier = (column(slot) == slot) & (down < along)
    rank = jnp.sum(jnp.where(earlier, 1.0, 0.0), axis=0, keepdims=True)
    at_row = slot * cap + rank
    at_col = column(at_row)
    select = (at_row == down.astype(f32)).astype(f32).astype(b16)
    unselect = (at_col == along.astype(f32)).astype(f32).astype(b16)
    is_even = lax.rem(lead, CORES) == 0
    by_core = [
        column(jnp.where(is_even, r.route_weight[k : k + 1, :], r.route_weight[1 - k : 2 - k, :]))
        for k in range(CORES)
    ]
    lane_at = lax.broadcasted_iota(jnp.int32, (tokens, 128), 1).astype(f32)
    row_at = lax.broadcasted_iota(jnp.int32, (8, 128), 0)
    for d in range(GROUPS):
        hit = at_col == lane_at + float(d * cap)
        picked = [jnp.sum(jnp.where(hit, by_core[k], 0.0), axis=0, keepdims=True) for k in range(CORES)]
        r.weights[d] = jnp.where(row_at == 0, picked[0], picked[1])
    for a, key in enumerate(("moe", "cot")):
        loads[key].wait()
        for n in range(4):
            cols = slice(n * width, (n + 1) * width)
            r.rows[a, :, :, cols] = (
                plain(select, getattr(r, "v_" + key)[:, cols]).astype(b16).reshape(GROUPS, cap, width)
            )
    for a in range(2):
        r.land[a, 0, c] = r.rows[a, 0]
    r.weight_in[0, c] = r.weights[0]
    loads["gate_c"].wait()
    loads["value_x"].wait()
    mixed = (r.v_gate_c[...].astype(f32) * r.v_value_x[...].astype(f32)).astype(b16).astype(f32)
    r.edge[...] = mixed[tokens - 8 :, :]
    pl.semaphore_wait(barrier, len(targets))

    steps = [(a, d) for d in range(1, GROUPS) for a in range(2)]
    copies = []

    def send(*args):
        copy = remote(*args)
        copy.start()
        copies.append(copy)
        return copy

    first, small = {}, {}
    for a, d in steps:
        first[a, d] = send(
            r.rows.at[a, d, :, mine],
            r.land.at[a, d, c, :, mine],
            r.sz.at[a, d - 1],
            r.rz.at[a, d - 1],
            peer[d],
        )
        if a == 0:
            small[d] = send(
                r.weights.at[d], r.weight_in.at[d, c], r.sw.at[d - 1], r.rw.at[d - 1], peer[d]
            )
    fourth, small_mate = {}, {}
    for a in range(2):
        fourth[a, 0] = send(
            r.rows.at[a, 0], r.land.at[a, 0, c], r.sm.at[a, 0], r.rm.at[a, 0], mate
        )
    small_mate[0] = send(
        r.weights.at[0], r.weight_in.at[0, c], r.sv.at[0], r.rv.at[0], mate
    )
    halo = send(r.edge, r.edge_in, r.sh.at[0], r.rh.at[0], after)

    second, third = {}, {}

    def e1(a, d):
        first[a, d].wait_recv()
        block = r.land.at[a, d, c, :, mine]
        for j in range(2):
            second[a, d, j] = send(block, block, r.sx.at[a, d - 1, j], r.rx.at[a, d - 1, j], lane[j])
        if a == 0:
            small[d].wait_recv()
            block = r.weight_in.at[d, c]
            small_mate[d] = send(block, block, r.sv.at[d], r.rv.at[d], mate)

    def e2(a, d):
        for j in range(2):
            second[a, d, j].wait_recv()
        for j in range(2):
            block = r.land.at[a, d, c, :, half(lanes[1 - j], j, width)]
            third[a, d, j] = send(block, block, r.sy.at[a, d - 1, j], r.ry.at[a, d - 1, j], lane[j])

    def e3(a, d):
        for j in range(2):
            third[a, d, j].wait_recv()
        block = r.land.at[a, d, c]
        fourth[a, d] = send(block, block, r.sm.at[a, d], r.rm.at[a, d], mate)

    def e4(a, d):
        fourth[a, d].wait_recv()

    cap_down = lax.broadcasted_iota(jnp.int32, (cap, 128), 0)
    cap_along = lax.broadcasted_iota(jnp.int32, (cap, 128), 1)

    def forward(d):
        small_mate[d].wait_recv()
        for k in range(CORES):
            tile = r.weight_in[d, k]
            row = jnp.sum(jnp.where(row_at == c, tile, 0.0), axis=0, keepdims=True)
            scale = jnp.sum(jnp.where(cap_down == cap_along, row, 0.0), axis=1, keepdims=True)
            r.scaled[d, k] = (scale * r.land[1, d, k].astype(f32)).astype(b16)
        x = r.land[0, d].reshape(CORES * cap, model)
        y = r.scaled[d].reshape(CORES * cap, model)
        for n in range(hid_rows // 256):
            hs = slice(n * 256, (n + 1) * 256)
            gate = last_dims(x, r.v_w_gate[hs, :])
            up = last_dims(x, r.v_w_up[hs, :])
            grad = last_dims(y, r.v_w_down[hs, :])
            sig = jax.nn.sigmoid(gate)
            silu = gate * sig
            r.hidden[d, :, hs] = (silu * up).astype(b16)
            r.gate_grad[d, :, hs] = (grad * up * sig * (1.0 + gate * (1.0 - sig))).astype(b16)
            r.up_grad[d, :, hs] = (grad * silu).astype(b16)

    swap, across, home, spread, relay = {}, {}, {}, {}, {}

    def backward(d):
        for n in range(4):
            cols = slice(n * width, (n + 1) * width)
            value = plain(r.gate_grad[d], r.v_w_gate[:, cols]) + plain(
                r.up_grad[d], r.v_w_up[:, cols]
            )
            r.part[d, :, :, cols] = value.astype(b16).reshape(CORES, cap, width)
        swap[d] = send(r.part.at[d, 1 - c], r.mate_in.at[d], r.sa.at[d], r.ra.at[d], mate)

    def reduce_start(d):
        swap[d].wait_recv()
        r.total[d] = (r.part[d, c].astype(f32) + r.mate_in[d].astype(f32)).astype(b16)
        for j in (2, 0, 1):
            across[d, j] = send(
                r.total.at[d, :, span(lanes[j], width)],
                r.lane_in.at[d, j],
                r.sb.at[d, j],
                r.rb.at[d, j],
                lane[j],
            )

    def spread_start(d):
        block = r.home.at[d, :, mine]
        for j in range(2):
            spread[d, j] = send(block, block, r.sd.at[d, j], r.rd.at[d, j], lane[j])

    def reduce_end(d):
        value = r.total[d, :, mine].astype(f32)
        for j in range(3):
            across[d, j].wait_recv()
            value = value + r.lane_in[d, j].astype(f32)
        if d == 0:
            r.home[0, :, mine] = value.astype(b16)
            spread_start(0)
        else:
            r.done[d - 1] = value.astype(b16)
            home[d] = send(
                r.done.at[d - 1], r.home.at[d, :, mine], r.sc.at[d - 1], r.rc.at[d - 1], peer[d]
            )

    def home_in(d):
        home[d].wait_recv()
        spread_start(d)

    def relay_start(d):
        for j in range(2):
            spread[d, j].wait_recv()
        for j in range(2):
            block = r.home.at[d, :, half(lanes[1 - j], j, width)]
            relay[d, j] = send(block, block, r.se.at[d, j], r.re.at[d, j], lane[j])

    def relay_end(d):
        for j in range(2):
            relay[d, j].wait_recv()

    sources = (("w_gate_grad", "gate_grad", 0), ("w_up_grad", "up_grad", 0), ("w_down_grad", "hidden", 1))

    def weight_grad(i):
        out, left, a = sources[i]
        lhs = getattr(r, left)[...].reshape(GROUPS * CORES * cap, hid_rows)
        for n in range(4):
            cols = slice(n * width, (n + 1) * width)
            rhs = r.land[0, :, :, :, cols] if a == 0 else r.scaled[:, :, :, cols]
            getattr(r, out)[:, cols] = first_dims(lhs, rhs.reshape(GROUPS * CORES * cap, width)).astype(b16)

    token_at = lax.broadcasted_iota(jnp.int32, (tokens, chan), 0)

    def conv_forward():
        halo.wait_recv()
        loads["taps"].wait()
        loads["gate_b"].wait()
        keep = jnp.where(s == 0, 0.0, 1.0)
        one, two = keep * r.edge_in[7:8, :], keep * r.edge_in[6:7, :]
        back_one = jnp.where(token_at == 0, one, pltpu.roll(mixed, 1, 0))
        back_two = jnp.where(
            token_at == 0, two, jnp.where(token_at == 1, one, pltpu.roll(mixed, 2, 0))
        )
        taps = r.v_taps
        conv = taps[0:1, :] * back_two + taps[1:2, :] * back_one + taps[2:3, :] * mixed
        r.conv[...] = conv
        act = (r.v_gate_b[...].astype(f32) * conv).astype(b16)
        unit = lax.broadcasted_iota(jnp.int32, (chan, chan), 0) == lax.broadcasted_iota(
            jnp.int32, (chan, chan), 1
        )
        r.act[...] = last_dims(unit.astype(f32).astype(b16), act).astype(b16)

    for key in ("w_gate", "w_up", "w_down"):
        loads[key].wait()
    e4(0, 0)
    e4(1, 0)
    forward(0)
    backward(0)
    e1(*steps[0])
    e1(*steps[1])
    reduce_start(0)
    e2(*steps[0])
    e1(*steps[2])
    e2(*steps[1])
    e3(*steps[0])
    conv_forward()
    e1(*steps[3])
    e2(*steps[2])
    e3(*steps[1])
    e4(*steps[0])
    e4(*steps[1])
    forward(1)
    e1(*steps[4])
    e2(*steps[3])
    e3(*steps[2])
    backward(1)
    e1(*steps[5])
    reduce_end(0)
    e2(*steps[4])
    e3(*steps[3])
    e4(*steps[2])
    e4(*steps[3])
    reduce_start(1)
    forward(2)
    e2(*steps[5])
    e3(*steps[4])
    backward(2)
    e3(*steps[5])
    reduce_start(2)
    e4(*steps[4])
    e4(*steps[5])
    forward(3)
    reduce_end(1)
    backward(3)
    relay_start(0)
    reduce_start(3)
    reduce_end(2)
    weight_grad(0)
    home_in(1)
    reduce_end(3)
    home_in(2)
    relay_start(1)
    weight_grad(1)
    home_in(3)
    relay_start(2)
    weight_grad(2)
    relay_start(3)
    loads["out_proj"].wait()
    for d in range(GROUPS):
        relay_end(d)

    for n in range(4):
        cols = slice(n * width, (n + 1) * width)
        full = plain(unselect, r.home[:, :, cols].reshape(tokens, width)).astype(b16)
        r.full[:, cols] = full
        r.stream[:, cols] = (r.v_cot[:, cols].astype(f32) + full.astype(f32)).astype(b16)
    narrow = width // CORES
    pair = {}
    act = r.act[...]
    for d in (2, 3, 1, 0):
        cols = span(CORES * far[d] + 1 - c, narrow)
        r.give[d] = plain(act, r.stream[:, cols]).astype(b16)
        pair[d] = send(r.give.at[d], r.take.at[d], r.sp.at[d], r.rp.at[d], mate)
    act_grad = last_dims(r.stream[...], r.v_out_proj[...])
    conv_grad = act_grad * r.v_gate_b[...].astype(f32)
    r.rim[...] = conv_grad[0:8, :]
    rim = send(r.rim, r.rim_in, r.sh.at[1], r.rh.at[1], before)
    wide = {}
    near = None
    for d in (2, 3, 1, 0):
        cols = span(CORES * far[d] + c, narrow)
        value = plain(act, r.stream[:, cols])
        pair[d].wait_recv()
        value = value + r.take[d].astype(f32)
        if d == 0:
            near = value
        else:
            r.sum[d - 1] = value.astype(b16)
            wide[d] = send(
                r.sum.at[d - 1], r.wide_in.at[d - 1], r.sq.at[d - 1], r.rq.at[d - 1], peer[d]
            )
    r.moe_in_grad[...] = r.full[:, mine]
    r.gate_b_grad[...] = (act_grad * r.conv[...]).astype(b16)
    rim.wait_recv()
    keep = jnp.where(s == devices - 1, 0.0, 1.0)
    one, two = keep * r.rim_in[0:1, :], keep * r.rim_in[1:2, :]
    next_one = jnp.where(token_at == tokens - 1, one, pltpu.roll(conv_grad, tokens - 1, 0))
    next_two = jnp.where(
        token_at == tokens - 1,
        two,
        jnp.where(token_at == tokens - 2, one, pltpu.roll(conv_grad, tokens - 2, 0)),
    )
    taps = r.v_taps
    mixed_grad = taps[0:1, :] * next_two + taps[1:2, :] * next_one + taps[2:3, :] * conv_grad
    r.gate_c_grad[...] = (mixed_grad * r.v_value_x[...].astype(f32)).astype(b16)
    r.value_x_grad[...] = (mixed_grad * r.v_gate_c[...].astype(f32)).astype(b16)
    for d in (1, 2, 3):
        wide[d].wait_recv()
        near = near + r.wide_in[d - 1].astype(f32)
    r.proj_grad[...] = near
    for copy in copies:
        copy.wait_send()


def store_kernel(*refs):
    count = len(refs) // 2
    copies = [pltpu.make_async_copy(refs[i], refs[count + i], refs[-1].at[i]) for i in range(count)]
    for copy in copies:
        copy.start()
    for copy in copies:
        copy.wait()


def on_device_paired(
    moe_in, cotangent, routing, route_weight, w_gate, w_up, w_down, gate_b, gate_c, value_x, conv_taps, out_proj
):
    tokens, model = moe_in.shape
    hid_rows = w_gate.shape[1]
    chan = gate_b.shape[0]
    cap, width = tokens // GROUPS, model // 4
    b16, f32 = moe_in.dtype, jnp.float32
    vmem, hbm = pl.BlockSpec(memory_space=pltpu.VMEM), pl.BlockSpec(memory_space=pltpu.HBM)
    dma = pltpu.SemaphoreType.DMA
    inputs = dict(
        routing=routing.T,
        route_weight=route_weight.T,
        moe=moe_in,
        cot=cotangent,
        w_gate=w_gate[0],
        w_up=w_up[0],
        w_down=w_down[0],
        gate_b=gate_b.T,
        gate_c=gate_c.T,
        value_x=value_x.T,
        taps=conv_taps,
        out_proj=out_proj,
    )
    outputs = dict(
        w_gate_grad=((hid_rows, model), b16),
        w_up_grad=((hid_rows, model), b16),
        w_down_grad=((hid_rows, model), b16),
        moe_in_grad=((tokens, width), b16),
        proj_grad=((chan, width // CORES), f32),
        gate_b_grad=((tokens, chan), b16),
        gate_c_grad=((tokens, chan), b16),
        value_x_grad=((tokens, chan), b16),
    )
    loaded = [key for key in inputs if key not in ("routing", "route_weight")]
    scratch = {"v_" + key: pltpu.VMEM(inputs[key].shape, inputs[key].dtype) for key in loaded}
    three, pair = GROUPS - 1, CORES * cap
    scratch |= dict(
        weights=pltpu.VMEM((GROUPS, 8, 128), f32),
        weight_in=pltpu.VMEM((GROUPS, CORES, 8, 128), f32),
        rows=pltpu.VMEM((2, GROUPS, cap, model), b16),
        land=pltpu.VMEM((2, GROUPS, CORES, cap, model), b16),
        scaled=pltpu.VMEM((GROUPS, CORES, cap, model), b16),
        hidden=pltpu.VMEM((GROUPS, pair, hid_rows), b16),
        gate_grad=pltpu.VMEM((GROUPS, pair, hid_rows), b16),
        up_grad=pltpu.VMEM((GROUPS, pair, hid_rows), b16),
        part=pltpu.VMEM((GROUPS, CORES, cap, model), b16),
        mate_in=pltpu.VMEM((GROUPS, cap, model), b16),
        total=pltpu.VMEM((GROUPS, cap, model), b16),
        lane_in=pltpu.VMEM((GROUPS, 3, cap, width), b16),
        done=pltpu.VMEM((three, cap, width), b16),
        home=pltpu.VMEM((GROUPS, cap, model), b16),
        full=pltpu.VMEM((tokens, model), b16),
        stream=pltpu.VMEM((tokens, model), b16),
        conv=pltpu.VMEM((tokens, chan), f32),
        act=pltpu.VMEM((chan, tokens), b16),
        edge=pltpu.VMEM((8, chan), f32),
        edge_in=pltpu.VMEM((8, chan), f32),
        rim=pltpu.VMEM((8, chan), f32),
        rim_in=pltpu.VMEM((8, chan), f32),
        give=pltpu.VMEM((GROUPS, chan, width // CORES), b16),
        take=pltpu.VMEM((GROUPS, chan, width // CORES), b16),
        sum=pltpu.VMEM((three, chan, width // CORES), b16),
        wide_in=pltpu.VMEM((three, chan, width // CORES), b16),
        load=dma((len(loaded),)),
    )
    counts = dict(
        z=(2, three),
        w=(three,),
        x=(2, three, 2),
        y=(2, three, 2),
        m=(2, GROUPS),
        v=(GROUPS,),
        h=(2,),
        a=(GROUPS,),
        b=(GROUPS, 3),
        c=(three,),
        d=(GROUPS, 2),
        e=(GROUPS, 2),
        p=(GROUPS,),
        q=(three,),
    )
    for key, shape in counts.items():
        scratch["s" + key] = dma(shape)
        scratch["r" + key] = dma(shape)
    names = list(inputs) + list(outputs) + list(scratch)
    out = pl.pallas_call(
        functools.partial(step_kernel, names),
        out_shape=tuple(pltpu.VMEM(*shape) for shape in outputs.values()),
        in_specs=[hbm if key in loaded else vmem for key in inputs],
        out_specs=(vmem,) * len(outputs),
        scratch_shapes=list(scratch.values()),
        compiler_params=pltpu.CompilerParams(
            collective_id=0, has_side_effects=True, vmem_limit_bytes=54 * 1024 * 1024
        ),
        name="step",
    )(*inputs.values())
    out = pl.pallas_call(
        store_kernel,
        out_shape=tuple(jax.ShapeDtypeStruct(*shape) for shape in outputs.values()),
        in_specs=[vmem] * len(outputs),
        out_specs=(hbm,) * len(outputs),
        scratch_shapes=[dma((len(outputs),))],
        compiler_params=pltpu.CompilerParams(vmem_limit_bytes=4 * 1024 * 1024),
        name="store",
    )(*out)
    out = types.SimpleNamespace(**dict(zip(outputs, out)))
    return (
        out.w_gate_grad[None],
        out.w_up_grad[None],
        out.w_down_grad[None],
        out.moe_in_grad,
        out.proj_grad,
        out.gate_b_grad.T,
        out.gate_c_grad.T,
        out.value_x_grad.T,
    )


def on_device(*args):
    routes = args[2].shape[1]
    experts, lane_count = lax.axis_size("sp"), lax.axis_size("tp")
    if experts == CORES * GROUPS and routes == CORES and lane_count == 4:
        return on_device_paired(*args)
    return on_device_general(*args)


def solution(mesh):
    in_specs = (
        P("sp", None),
        P("sp", None),
        P("sp", None),
        P("sp", None),
        P("sp", "tp", None),
        P("sp", "tp", None),
        P("sp", "tp", None),
        P("tp", "sp"),
        P("tp", "sp"),
        P("tp", "sp"),
        P(None, "tp"),
        P("tp", None),
    )
    out_specs = (
        P("sp", "tp", None),
        P("sp", "tp", None),
        P("sp", "tp", None),
        P("sp", "tp"),
        P("tp", "sp"),
        P("tp", "sp"),
        P("tp", "sp"),
        P("tp", "sp"),
    )
    return jax.shard_map(
        on_device, mesh=mesh, in_specs=in_specs, out_specs=out_specs, check_vma=False
    )
```

time: 107 us -> 69.7 us (0.65)
  matrix products: 21.5 us -> 0 us
  other arithmetic: 5.23 us -> 0 us
  Pallas kernels: 73.9 us -> 68.8 us
  starting transfers between devices: 3.68 us -> 0 us
  local copies, waits for them, and re-layouts: 1.77 us -> 0 us
    dot_general x11 -> x0, matrix products: 21.5 us -> none  [the longest x1 2.67 us: on_device_paired(): lax.dot_general(hidden, arrived_cot, over_rows, preferred_element_type=jn...]
    pallas_call x3 -> x2, Pallas kernels: 73.9 us -> 68.8 us  [the longest x1 65.9 us: on_device_paired(): pl.pallas_call(functools.partial(step_kernel, names), out_shape=tuple((pl...]
    ppermute x2 -> x0, starting transfers between devices: 3.68 us -> none  [from_behind(): return lax.ppermute(array, axis, pairs)]
    convert_element_type x4 -> x0, other arithmetic: 2.53 us -> none  [the longest x1 1.12 us: on_device_paired(): (gate_c.astype(jnp.float32) * value_x.astype(jnp.float32)).astype(jnp.bfl...]
    add x2 -> x0, other arithmetic: 1.89 us -> none  [the longest x1 1.87 us: on_device_paired(): near + (far[0].astype(jnp.float32) + far[1].astype(jnp.float32))]
  transfers between devices with their start and end apart: 2 -> 0, of which waited for: 0 -> 0; matrix products, arithmetic and copies ran while one was open for 21% -> 0% of each run, Pallas kernels for 69% -> 0%
where the time goes in v1:
time: 69.7 us; the launch traced here: 69.5 us
  Pallas kernels  68.8 us (99%)
    pallas_call x1, Pallas kernels, on_device_paired(): pl.pallas_call(functools.partial(step_kernel, names), out_shape=tuple((pl...  65.9 us
    pallas_call x1, Pallas kernels, on_device_paired(): pl.pallas_call(store_kernel, out_shape=tuple((jax.ShapeDtypeStruct(*shape...  2.92 us

profile of v1, /device:TPU:0, one launch (start us, length us, event | category | flops | bytes accessed | tf_op | source)
XLA Modules:
  0.0 69.5 jit_solution(10774745679231173310)
XLA Ops:
  0.6 65.9 %step.1 = (bf16[512,2048]{1,0:T(8,128)(2,1)S(1)}, bf16[512,2048]{1,0:T(8,128)(2,1)S(1)}, bf16[512,2048]{1,0:T(8,128)(2,1)S(1)}, bf16[192,512]{1,0:T(8,128)(2,1)S...) custom-call(s32[2,192]{1,0:T(2,128)} %bitcast.20, ...), custom_call_target="tpu_custom_call" | custom-call | tf_op jit(solution)/shard_map/step/pallas_call | solution.py:645
  66.5 2.9 %store.1 = (bf16[512,2048]{1,0:T(8,128)(2,1)}, bf16[512,2048]{1,0:T(8,128)(2,1)}, bf16[512,2048]{1,0:T(8,128)(2,1)}, bf16[192,512]{1,0:T(8,128)(2,1)}, f32[256,2...) custom-call(bf16[512,2048]{1,0:T(8,128)(2,1)S(1)} %get-tuple-element.24.refs_0_, ...), custom_call_target="tpu_custom_call" | custom-call | tf_op jit(solution)/shard_map/store/pallas_call | solution.py:656

commit v2 on v1

--- a/solution.py
+++ b/solution.py
@@ -207,6 +207,8 @@
     side = (CORES * side_z + 1 - c, t)
     lane = [(s, lanes[j]) for j in range(3)]
     mine = span(t, width)
+    sub = width // 4
+    mine_sub = span(t, sub)
 
     loads = {}
     order = ("moe", "cot", "gate_c", "value_x", "w_gate", "w_up", "w_down", "gate_b", "taps", "out_proj")
@@ -236,7 +238,42 @@
     at_row = slot * cap + rank
     at_col = column(at_row)
     select = (at_row == down.astype(f32)).astype(f32).astype(b16)
+    r.pick[...] = select
     unselect = (at_col == along.astype(f32)).astype(f32).astype(b16)
+    for a, key in enumerate(("moe", "cot")):
+        loads[key].wait()
+        for n in range(4):
+            cols = slice(n * width, (n + 1) * width)
+            r.rows[a, :, :, cols] = (
+                plain(select, getattr(r, "v_" + key)[:, cols]).astype(b16).reshape(GROUPS, cap, width)
+            )
+    for a in range(2):
+        r.land[a, 0, c] = r.rows[a, 0]
+    pl.semaphore_wait(barrier, len(targets))
+
+    steps = [(a, d) for d in range(1, GROUPS) for a in range(2)]
+    copies = []
+
+    def send(*args):
+        copy = remote(*args)
+        copy.start()
+        copies.append(copy)
+        return copy
+
+    first, small = {}, {}
+    for a, d in steps[:2]:
+        first[a, d] = send(
+            r.rows.at[a, d, :, mine],
+            r.land.at[a, d, c, :, mine],
+            r.sz.at[a, d - 1],
+            r.rz.at[a, d - 1],
+            peer[d],
+        )
+    fourth, small_mate = {}, {}
+    for a in range(2):
+        fourth[a, 0] = send(
+            r.rows.at[a, 0], r.land.at[a, 0, c], r.sm.at[a, 0], r.rm.at[a, 0], mate
+        )
     is_even = lax.rem(lead, CORES) == 0
     by_core = [
         column(jnp.where(is_even, r.route_weight[k : k + 1, :], r.route_weight[1 - k : 2 - k, :]))
@@ -248,33 +285,19 @@
         hit = at_col == lane_at + float(d * cap)
         picked = [jnp.sum(jnp.where(hit, by_core[k], 0.0), axis=0, keepdims=True) for k in range(CORES)]
         r.weights[d] = jnp.where(row_at == 0, picked[0], picked[1])
-    for a, key in enumerate(("moe", "cot")):
-        loads[key].wait()
-        for n in range(4):
-            cols = slice(n * width, (n + 1) * width)
-            r.rows[a, :, :, cols] = (
-                plain(select, getattr(r, "v_" + key)[:, cols]).astype(b16).reshape(GROUPS, cap, width)
-            )
-    for a in range(2):
-        r.land[a, 0, c] = r.rows[a, 0]
     r.weight_in[0, c] = r.weights[0]
+    for d in range(1, GROUPS):
+        small[d] = send(r.weights.at[d], r.weight_in.at[d, c], r.sw.at[d - 1], r.rw.at[d - 1], peer[d])
+    small_mate[0] = send(
+        r.weights.at[0], r.weight_in.at[0, c], r.sv.at[0], r.rv.at[0], mate
+    )
     loads["gate_c"].wait()
     loads["value_x"].wait()
     mixed = (r.v_gate_c[...].astype(f32) * r.v_value_x[...].astype(f32)).astype(b16).astype(f32)
     r.edge[...] = mixed[tokens - 8 :, :]
-    pl.semaphore_wait(barrier, len(targets))
-
-    steps = [(a, d) for d in range(1, GROUPS) for a in range(2)]
-    copies = []
-
-    def send(*args):
-        copy = remote(*args)
-        copy.start()
-        copies.append(copy)
-        return copy
-
-    first, small = {}, {}
-    for a, d in steps:
+    halo = send(r.edge, r.edge_in, r.sh.at[0], r.rh.at[0], after)
+
+    for a, d in steps[2:]:
         first[a, d] = send(
             r.rows.at[a, d, :, mine],
             r.land.at[a, d, c, :, mine],
@@ -282,19 +305,6 @@
             r.rz.at[a, d - 1],
             peer[d],
         )
-        if a == 0:
-            small[d] = send(
-                r.weights.at[d], r.weight_in.at[d, c], r.sw.at[d - 1], r.rw.at[d - 1], peer[d]
-            )
-    fourth, small_mate = {}, {}
-    for a in range(2):
-        fourth[a, 0] = send(
-            r.rows.at[a, 0], r.land.at[a, 0, c], r.sm.at[a, 0], r.rm.at[a, 0], mate
-        )
-    small_mate[0] = send(
-        r.weights.at[0], r.weight_in.at[0, c], r.sv.at[0], r.rv.at[0], mate
-    )
-    halo = send(r.edge, r.edge_in, r.sh.at[0], r.rh.at[0], after)
 
     second, third = {}, {}
 
@@ -303,7 +313,7 @@
         block = r.land.at[a, d, c, :, mine]
         for j in range(2):
             second[a, d, j] = send(block, block, r.sx.at[a, d - 1, j], r.rx.at[a, d - 1, j], lane[j])
-        if a == 0:
+        if a == 1:
             small[d].wait_recv()
             block = r.weight_in.at[d, c]
             small_mate[d] = send(block, block, r.sv.at[d], r.rv.at[d], mate)
@@ -326,6 +336,18 @@
 
     cap_down = lax.broadcasted_iota(jnp.int32, (cap, 128), 0)
     cap_along = lax.broadcasted_iota(jnp.int32, (cap, 128), 1)
+
+    unit = lax.broadcasted_iota(jnp.int32, (256, 256), 0) == lax.broadcasted_iota(
+        jnp.int32, (256, 256), 1
+    )
+    r.unit[...] = unit.astype(f32).astype(b16)
+    turns = ("w_gate", "w_up", "w_down")
+
+    def turn(i, first_tile, count):
+        source, out = getattr(r, "v_" + turns[i]), r.turned
+        for n in range(first_tile, first_tile + count):
+            at = slice(n * 256, (n + 1) * 256)
+            out[i, at, :] = last_dims(r.unit[...], source[:, at]).astype(b16)
 
     def forward(d):
         small_mate[d].wait_recv()
@@ -336,18 +358,25 @@
             r.scaled[d, k] = (scale * r.land[1, d, k].astype(f32)).astype(b16)
         x = r.land[0, d].reshape(CORES * cap, model)
         y = r.scaled[d].reshape(CORES * cap, model)
-        for n in range(hid_rows // 256):
-            hs = slice(n * 256, (n + 1) * 256)
-            gate = last_dims(x, r.v_w_gate[hs, :])
-            up = last_dims(x, r.v_w_up[hs, :])
-            grad = last_dims(y, r.v_w_down[hs, :])
+        block = hid_rows // 2
+        for n in range(2):
+            hs = slice(n * block, (n + 1) * block)
+            if d == 0:
+                gate = last_dims(x, r.v_w_gate[hs, :])
+                up = last_dims(x, r.v_w_up[hs, :])
+                grad = last_dims(y, r.v_w_down[hs, :])
+            else:
+                gate = plain(x, r.turned[0, :, hs])
+                up = plain(x, r.turned[1, :, hs])
+                grad = plain(y, r.turned[2, :, hs])
             sig = jax.nn.sigmoid(gate)
             silu = gate * sig
             r.hidden[d, :, hs] = (silu * up).astype(b16)
             r.gate_grad[d, :, hs] = (grad * up * sig * (1.0 + gate * (1.0 - sig))).astype(b16)
             r.up_grad[d, :, hs] = (grad * silu).astype(b16)
 
-    swap, across, home, spread, relay = {}, {}, {}, {}, {}
+    swap, across, hop, home, spread, relay = {}, {}, {}, {}, {}, {}
+    piece, fan, pass_on = {}, {}, {}
 
     def backward(d):
         for n in range(4):
@@ -355,20 +384,31 @@
             value = plain(r.gate_grad[d], r.v_w_gate[:, cols]) + plain(
                 r.up_grad[d], r.v_w_up[:, cols]
             )
-            r.part[d, :, :, cols] = value.astype(b16).reshape(CORES, cap, width)
+            value = value.astype(b16).reshape(CORES, cap, width)
+            for q in range(4):
+                at = q * width + n * sub
+                r.part[d, :, :, at : at + sub] = value[:, :, q * sub : (q + 1) * sub]
         swap[d] = send(r.part.at[d, 1 - c], r.mate_in.at[d], r.sa.at[d], r.ra.at[d], mate)
 
     def reduce_start(d):
         swap[d].wait_recv()
         r.total[d] = (r.part[d, c].astype(f32) + r.mate_in[d].astype(f32)).astype(b16)
-        for j in (2, 0, 1):
-            across[d, j] = send(
-                r.total.at[d, :, span(lanes[j], width)],
-                r.lane_in.at[d, j],
-                r.sb.at[d, j],
-                r.rb.at[d, j],
-                lane[j],
-            )
+        for j in range(2):
+            for i, target in enumerate((2, j)):
+                across[d, j, 1 - i] = send(
+                    r.total.at[d, :, half(lanes[target], j, width)],
+                    r.lane_in.at[d, j, 1 - i],
+                    r.sb.at[d, j, 1 - i],
+                    r.rb.at[d, j, 1 - i],
+                    lane[j],
+                )
+
+    def reduce_mid(d):
+        for j in range(2):
+            across[d, j, 1].wait_recv()
+            value = r.total[d, :, half(lanes[1 - j], j, width)].astype(f32) + r.lane_in[d, j, 1].astype(f32)
+            r.hop[d, j] = value.astype(b16)
+            hop[d, j] = send(r.hop.at[d, j], r.hop_in.at[d, j], r.sg.at[d, j], r.rg.at[d, j], lane[1 - j])
 
     def spread_start(d):
         block = r.home.at[d, :, mine]
@@ -376,18 +416,51 @@
             spread[d, j] = send(block, block, r.sd.at[d, j], r.rd.at[d, j], lane[j])
 
     def reduce_end(d):
-        value = r.total[d, :, mine].astype(f32)
-        for j in range(3):
-            across[d, j].wait_recv()
-            value = value + r.lane_in[d, j].astype(f32)
+        for j in range(2):
+            across[d, j, 0].wait_recv()
+            hop[d, j].wait_recv()
+            value = r.total[d, :, half(t, j, width)].astype(f32) + r.lane_in[d, j, 0].astype(f32)
+            value = value + r.hop_in[d, j].astype(f32)
+            r.done[d, :, j * (width // 2) : (j + 1) * (width // 2)] = value.astype(b16)
+        if d > 0:
+            home[d] = send(
+                r.done.at[d], r.home.at[d, :, mine], r.sc.at[d - 1], r.rc.at[d - 1], peer[d]
+            )
+        for e in (3, 2, 1, 0):
+            own = pl.ds(pl.multiple_of(far[e] * width + t * sub, sub), sub)
+            value = r.land[1, d, c, :, own].astype(f32) + r.done[d, :, span(far[e], sub)].astype(f32)
+            if e > 0:
+                r.op_out[d, e - 1] = value.astype(b16)
+                piece[d, e] = send(
+                    r.op_out.at[d, e - 1],
+                    r.op.at[e, d, :, mine_sub],
+                    r.sp.at[d, e - 1],
+                    r.rp.at[d, e - 1],
+                    peer[e],
+                )
+            else:
+                r.op[0, d, :, mine_sub] = value.astype(b16)
         if d == 0:
-            r.home[0, :, mine] = value.astype(b16)
+            r.home[0, :, mine] = r.done[0]
             spread_start(0)
-        else:
-            r.done[d - 1] = value.astype(b16)
-            home[d] = send(
-                r.done.at[d - 1], r.home.at[d, :, mine], r.sc.at[d - 1], r.rc.at[d - 1], peer[d]
-            )
+
+    def fan_start(d):
+        for e in range(1, GROUPS):
+            piece[d, e].wait_recv()
+        block = r.op.at[:, d, :, mine_sub]
+        for j in range(2):
+            fan[d, j] = send(block, block, r.sq.at[d, j], r.rq.at[d, j], lane[j])
+
+    def pass_start(d):
+        for j in range(2):
+            fan[d, j].wait_recv()
+        for j in range(2):
+            block = r.op.at[2 * j : 2 * j + 2, d, :, span(lanes[1 - j], sub)]
+            pass_on[d, j] = send(block, block, r.so.at[d, j], r.ro.at[d, j], lane[j])
+
+    def pass_end(d):
+        for j in range(2):
+            pass_on[d, j].wait_recv()
 
     def home_in(d):
         home[d].wait_recv()
@@ -406,10 +479,10 @@
 
     sources = (("w_gate_grad", "gate_grad", 0), ("w_up_grad", "up_grad", 0), ("w_down_grad", "hidden", 1))
 
-    def weight_grad(i):
+    def weight_grad(i, *tiles):
         out, left, a = sources[i]
         lhs = getattr(r, left)[...].reshape(GROUPS * CORES * cap, hid_rows)
-        for n in range(4):
+        for n in tiles:
             cols = slice(n * width, (n + 1) * width)
             rhs = r.land[0, :, :, :, cols] if a == 0 else r.scaled[:, :, :, cols]
             getattr(r, out)[:, cols] = first_dims(lhs, rhs.reshape(GROUPS * CORES * cap, width)).astype(b16)
@@ -430,103 +503,157 @@
         conv = taps[0:1, :] * back_two + taps[1:2, :] * back_one + taps[2:3, :] * mixed
         r.conv[...] = conv
         act = (r.v_gate_b[...].astype(f32) * conv).astype(b16)
-        unit = lax.broadcasted_iota(jnp.int32, (chan, chan), 0) == lax.broadcasted_iota(
-            jnp.int32, (chan, chan), 1
-        )
-        r.act[...] = last_dims(unit.astype(f32).astype(b16), act).astype(b16)
-
-    for key in ("w_gate", "w_up", "w_down"):
-        loads[key].wait()
+        r.act_in[0] = plain(r.pick[...], act).astype(b16).reshape(GROUPS, cap, chan)
+
+    action = {}
+
+    def act_start():
+        for d in (3, 2, 1):
+            action[d] = send(
+                r.act_in.at[0], r.act_in.at[d], r.su.at[d - 1], r.ru.at[d - 1], peer[d]
+            )
+
+    def stream_of(pull, n):
+        slabs = [r.home[:, :, q * width + n * sub : q * width + (n + 1) * sub] for q in range(4)]
+        slab = jnp.concatenate(slabs, axis=2).reshape(tokens, width)
+        return plain(pull, slab).astype(b16)
+
+    last = {}
+
+    def rim_start():
+        for d in range(GROUPS):
+            relay_end(d)
+        loads["out_proj"].wait()
+        for n in range(4):
+            cols = slice(n * width, (n + 1) * width)
+            full = stream_of(unselect[0:16, :], n)
+            r.stream[0:16, cols] = (r.v_cot[0:16, cols].astype(f32) + full.astype(f32)).astype(b16)
+        top = last_dims(r.stream[0:16, :], r.v_out_proj[...])[0:8, :]
+        r.rim[...] = top * r.v_gate_b[0:16, :].astype(f32)[0:8, :]
+        last[0] = send(r.rim, r.rim_in, r.sh.at[1], r.rh.at[1], before)
+
+    def project():
+        for d in range(1, GROUPS):
+            action[d].wait_recv()
+        for e in range(GROUPS):
+            for d in range(GROUPS):
+                r.mix[e, d] = r.act_in[e ^ d, d]
+        for d in range(GROUPS):
+            pass_end(d)
+        narrow = width // CORES
+        rows_all = GROUPS * GROUPS * cap
+        mix = r.mix[...].reshape(rows_all, chan)
+        there = r.op[:, :, :, span(1 - c, narrow)].reshape(rows_all, narrow)
+        r.give[...] = first_dims(mix, there).astype(b16)
+        last[1] = send(r.give, r.take, r.sn.at[0], r.rn.at[0], mate)
+        here = r.op[:, :, :, span(c, narrow)].reshape(rows_all, narrow)
+        r.proj_grad[...] = first_dims(mix, here)
+
+    def stream_all():
+        for n in range(4):
+            cols = slice(n * width, (n + 1) * width)
+            full = stream_of(unselect, n)
+            r.full[:, cols] = full
+            r.stream[:, cols] = (r.v_cot[:, cols].astype(f32) + full.astype(f32)).astype(b16)
+
+    loads["w_gate"].wait()
+    loads["w_up"].wait()
+    loads["w_down"].wait()
+    turn(1, 6, 2)
     e4(0, 0)
     e4(1, 0)
     forward(0)
-    backward(0)
     e1(*steps[0])
     e1(*steps[1])
+    turn(1, 2, 2)
+    e1(*steps[2])
+    backward(0)
+    e1(*steps[3])
+    turn(1, 4, 2)
+    turn(0, 0, 2)
+    conv_forward()
+    e2(*steps[0])
+    turn(2, 2, 2)
+    e2(*steps[1])
+    turn(2, 6, 2)
+    e1(*steps[4])
+    turn(0, 2, 2)
+    e2(*steps[2])
+    e2(*steps[3])
+    e1(*steps[5])
+    turn(0, 6, 2)
+    turn(0, 4, 2)
+    act_start()
+    turn(1, 0, 2)
+    turn(2, 4, 2)
+    e3(*steps[1])
+    e3(*steps[0])
     reduce_start(0)
-    e2(*steps[0])
-    e1(*steps[2])
-    e2(*steps[1])
-    e3(*steps[0])
-    conv_forward()
-    e1(*steps[3])
-    e2(*steps[2])
-    e3(*steps[1])
-    e4(*steps[0])
-    e4(*steps[1])
+    e3(*steps[2])
+    e2(*steps[4])
+    turn(2, 0, 2)
+    e3(*steps[3])
+    e4(0, 1)
+    e4(1, 1)
     forward(1)
-    e1(*steps[4])
-    e2(*steps[3])
-    e3(*steps[2])
+    e2(*steps[5])
     backward(1)
-    e1(*steps[5])
-    reduce_end(0)
-    e2(*steps[4])
-    e3(*steps[3])
-    e4(*steps[2])
-    e4(*steps[3])
-    reduce_start(1)
+    reduce_mid(0)
+    e4(0, 2)
+    e4(1, 2)
     forward(2)
-    e2(*steps[5])
     e3(*steps[4])
     backward(2)
+    reduce_start(1)
     e3(*steps[5])
     reduce_start(2)
-    e4(*steps[4])
-    e4(*steps[5])
+    reduce_end(0)
+    e4(0, 3)
+    e4(1, 3)
     forward(3)
+    backward(3)
+    reduce_mid(1)
+    weight_grad(0, 2)
+    reduce_mid(2)
+    reduce_start(3)
     reduce_end(1)
-    backward(3)
+    fan_start(0)
+    reduce_end(2)
+    reduce_mid(3)
     relay_start(0)
-    reduce_start(3)
-    reduce_end(2)
-    weight_grad(0)
     home_in(1)
+    fan_start(1)
     reduce_end(3)
+    weight_grad(2, 3)
+    weight_grad(2, 0)
+    pass_start(0)
+    weight_grad(1, 0)
     home_in(2)
     relay_start(1)
-    weight_grad(1)
+    weight_grad(1, 2)
+    weight_grad(0, 1)
+    pass_start(1)
+    fan_start(2)
+    weight_grad(0, 3)
     home_in(3)
+    fan_start(3)
+    weight_grad(1, 1)
     relay_start(2)
-    weight_grad(2)
+    weight_grad(0, 0)
+    weight_grad(1, 3)
+    weight_grad(2, 2)
+    pass_start(2)
     relay_start(3)
-    loads["out_proj"].wait()
-    for d in range(GROUPS):
-        relay_end(d)
-
-    for n in range(4):
-        cols = slice(n * width, (n + 1) * width)
-        full = plain(unselect, r.home[:, :, cols].reshape(tokens, width)).astype(b16)
-        r.full[:, cols] = full
-        r.stream[:, cols] = (r.v_cot[:, cols].astype(f32) + full.astype(f32)).astype(b16)
-    narrow = width // CORES
-    pair = {}
-    act = r.act[...]
-    for d in (2, 3, 1, 0):
-        cols = span(CORES * far[d] + 1 - c, narrow)
-        r.give[d] = plain(act, r.stream[:, cols]).astype(b16)
-        pair[d] = send(r.give.at[d], r.take.at[d], r.sp.at[d], r.rp.at[d], mate)
+    weight_grad(2, 1)
+    pass_start(3)
+    rim_start()
+    project()
+    stream_all()
     act_grad = last_dims(r.stream[...], r.v_out_proj[...])
     conv_grad = act_grad * r.v_gate_b[...].astype(f32)
-    r.rim[...] = conv_grad[0:8, :]
-    rim = send(r.rim, r.rim_in, r.sh.at[1], r.rh.at[1], before)
-    wide = {}
-    near = None
-    for d in (2, 3, 1, 0):
-        cols = span(CORES * far[d] + c, narrow)
-        value = plain(act, r.stream[:, cols])
-        pair[d].wait_recv()
-        value = value + r.take[d].astype(f32)
-        if d == 0:
-            near = value
-        else:
-            r.sum[d - 1] = value.astype(b16)
-            wide[d] = send(
-                r.sum.at[d - 1], r.wide_in.at[d - 1], r.sq.at[d - 1], r.rq.at[d - 1], peer[d]
-            )
     r.moe_in_grad[...] = r.full[:, mine]
     r.gate_b_grad[...] = (act_grad * r.conv[...]).astype(b16)
-    rim.wait_recv()
+    last[0].wait_recv()
     keep = jnp.where(s == devices - 1, 0.0, 1.0)
     one, two = keep * r.rim_in[0:1, :], keep * r.rim_in[1:2, :]
     next_one = jnp.where(token_at == tokens - 1, one, pltpu.roll(conv_grad, tokens - 1, 0))
@@ -539,10 +666,8 @@
     mixed_grad = taps[0:1, :] * next_two + taps[1:2, :] * next_one + taps[2:3, :] * conv_grad
     r.gate_c_grad[...] = (mixed_grad * r.v_value_x[...].astype(f32)).astype(b16)
     r.value_x_grad[...] = (mixed_grad * r.v_gate_c[...].astype(f32)).astype(b16)
-    for d in (1, 2, 3):
-        wide[d].wait_recv()
-        near = near + r.wide_in[d - 1].astype(f32)
-    r.proj_grad[...] = near
+    last[1].wait_recv()
+    r.proj_grad[...] = r.proj_grad[...] + r.take[...].astype(f32)
     for copy in copies:
         copy.wait_send()
 
@@ -605,21 +730,27 @@
         part=pltpu.VMEM((GROUPS, CORES, cap, model), b16),
         mate_in=pltpu.VMEM((GROUPS, cap, model), b16),
         total=pltpu.VMEM((GROUPS, cap, model), b16),
-        lane_in=pltpu.VMEM((GROUPS, 3, cap, width), b16),
-        done=pltpu.VMEM((three, cap, width), b16),
+        lane_in=pltpu.VMEM((GROUPS, 2, 2, cap, width // 2), b16),
+        done=pltpu.VMEM((GROUPS, cap, width), b16),
         home=pltpu.VMEM((GROUPS, cap, model), b16),
         full=pltpu.VMEM((tokens, model), b16),
         stream=pltpu.VMEM((tokens, model), b16),
         conv=pltpu.VMEM((tokens, chan), f32),
-        act=pltpu.VMEM((chan, tokens), b16),
         edge=pltpu.VMEM((8, chan), f32),
         edge_in=pltpu.VMEM((8, chan), f32),
         rim=pltpu.VMEM((8, chan), f32),
         rim_in=pltpu.VMEM((8, chan), f32),
-        give=pltpu.VMEM((GROUPS, chan, width // CORES), b16),
-        take=pltpu.VMEM((GROUPS, chan, width // CORES), b16),
-        sum=pltpu.VMEM((three, chan, width // CORES), b16),
-        wide_in=pltpu.VMEM((three, chan, width // CORES), b16),
+        give=pltpu.VMEM((chan, width // CORES), b16),
+        take=pltpu.VMEM((chan, width // CORES), b16),
+        unit=pltpu.VMEM((256, 256), b16),
+        turned=pltpu.VMEM((3, model, hid_rows), b16),
+        pick=pltpu.VMEM((tokens, tokens), b16),
+        hop=pltpu.VMEM((GROUPS, 2, cap, width // 2), b16),
+        hop_in=pltpu.VMEM((GROUPS, 2, cap, width // 2), b16),
+        op=pltpu.VMEM((GROUPS, GROUPS, cap, width), b16),
+        op_out=pltpu.VMEM((GROUPS, three, cap, width // 4), b16),
+        act_in=pltpu.VMEM((GROUPS, GROUPS, cap, chan), b16),
+        mix=pltpu.VMEM((GROUPS, GROUPS, cap, chan), b16),
         load=dma((len(loaded),)),
     )
     counts = dict(
@@ -631,12 +762,16 @@
         v=(GROUPS,),
         h=(2,),
         a=(GROUPS,),
-        b=(GROUPS, 3),
+        b=(GROUPS, 2, 2),
+        g=(GROUPS, 2),
         c=(three,),
         d=(GROUPS, 2),
         e=(GROUPS, 2),
-        p=(GROUPS,),
-        q=(three,),
+        p=(GROUPS, three),
+        q=(GROUPS, 2),
+        o=(GROUPS, 2),
+        u=(three,),
+        n=(1,),
     )
     for key, shape in counts.items():
         scratch["s" + key] = dma(shape)

time: 69.7 us -> 57.5 us (0.82)
  Pallas kernels: 68.8 us -> 56.5 us
    pallas_call x1, Pallas kernels: 65.9 us -> 53.5 us  [on_device_paired(): pl.pallas_call(functools.partial(step_kernel, names), out_shape=tuple((pl...]
where the time goes in v2:
time: 57.5 us; the launch traced here: 57.3 us
  Pallas kernels  56.5 us (98%)
  between operations  0.81 us (1%)
    pallas_call x1, Pallas kernels, on_device_paired(): pl.pallas_call(functools.partial(step_kernel, names), out_shape=tuple((pl...  53.5 us
    pallas_call x1, Pallas kernels, on_device_paired(): pl.pallas_call(store_kernel, out_shape=tuple((jax.ShapeDtypeStruct(*shape...  2.92 us

profile of v2, /device:TPU:0, one launch (start us, length us, event | category | flops | bytes accessed | tf_op | source)
XLA Modules:
  0.0 57.3 jit_solution(2896256314721690296)
XLA Ops:
  0.6 53.5 %step.1 = (bf16[512,2048]{1,0:T(8,128)(2,1)S(1)}, bf16[512,2048]{1,0:T(8,128)(2,1)S(1)}, bf16[512,2048]{1,0:T(8,128)(2,1)S(1)}, bf16[192,512]{1,0:T(8,128)(2,1)S...) custom-call(s32[2,192]{1,0:T(2,128)} %bitcast.20, ...), custom_call_target="tpu_custom_call" | custom-call | tf_op jit(solution)/shard_map/step/pallas_call | solution.py:780
  54.2 2.9 %store.1 = (bf16[512,2048]{1,0:T(8,128)(2,1)}, bf16[512,2048]{1,0:T(8,128)(2,1)}, bf16[512,2048]{1,0:T(8,128)(2,1)}, bf16[192,512]{1,0:T(8,128)(2,1)}, f32[256,2...) custom-call(bf16[512,2048]{1,0:T(8,128)(2,1)S(1)} %get-tuple-element.24.refs_0_, ...), custom_call_target="tpu_custom_call" | custom-call | tf_op jit(solution)/shard_map/store/pallas_call | solution.py:791

commit v3 on v2

--- a/solution.py
+++ b/solution.py
@@ -211,7 +211,7 @@
     mine_sub = span(t, sub)
 
     loads = {}
-    order = ("moe", "cot", "gate_c", "value_x", "w_gate", "w_up", "w_down", "gate_b", "taps", "out_proj")
+    order = ("routing", "route_weight", "moe", "cot", "gate_c", "value_x", "w_gate", "w_up", "w_down", "gate_b", "taps", "out_proj")
     for i, key in enumerate(order):
         loads[key] = pltpu.make_async_copy(getattr(r, key), getattr(r, "v_" + key), r.load.at[i])
         loads[key].start()
@@ -227,7 +227,8 @@
     def column(row):
         return jnp.sum(jnp.where(eye, row, 0.0), axis=1, keepdims=True)
 
-    lead = r.routing[0:1, :]
+    loads["routing"].wait()
+    lead = r.v_routing[0:1, :]
     group = lax.div(lead, CORES)
     low, high = lax.rem(group, 2), lax.div(group, 2)
     z_low, z_high = lax.rem(z, 2), lax.div(z, 2)
@@ -274,9 +275,10 @@
         fourth[a, 0] = send(
             r.rows.at[a, 0], r.land.at[a, 0, c], r.sm.at[a, 0], r.rm.at[a, 0], mate
         )
+    loads["route_weight"].wait()
     is_even = lax.rem(lead, CORES) == 0
     by_core = [
-        column(jnp.where(is_even, r.route_weight[k : k + 1, :], r.route_weight[1 - k : 2 - k, :]))
+        column(jnp.where(is_even, r.v_route_weight[k : k + 1, :], r.v_route_weight[1 - k : 2 - k, :]))
         for k in range(CORES)
     ]
     lane_at = lax.broadcasted_iota(jnp.int32, (tokens, 128), 1).astype(f32)
@@ -313,23 +315,23 @@
         block = r.land.at[a, d, c, :, mine]
         for j in range(2):
             second[a, d, j] = send(block, block, r.sx.at[a, d - 1, j], r.rx.at[a, d - 1, j], lane[j])
+
+    def e2(a, d):
+        for j in range(2):
+            second[a, d, j].wait_recv()
+        for j in range(2):
+            block = r.land.at[a, d, c, :, half(lanes[1 - j], j, width)]
+            third[a, d, j] = send(block, block, r.sy.at[a, d - 1, j], r.ry.at[a, d - 1, j], lane[j])
+
+    def e3(a, d):
+        for j in range(2):
+            third[a, d, j].wait_recv()
+        block = r.land.at[a, d, c]
+        fourth[a, d] = send(block, block, r.sm.at[a, d], r.rm.at[a, d], mate)
         if a == 1:
             small[d].wait_recv()
             block = r.weight_in.at[d, c]
             small_mate[d] = send(block, block, r.sv.at[d], r.rv.at[d], mate)
-
-    def e2(a, d):
-        for j in range(2):
-            second[a, d, j].wait_recv()
-        for j in range(2):
-            block = r.land.at[a, d, c, :, half(lanes[1 - j], j, width)]
-            third[a, d, j] = send(block, block, r.sy.at[a, d - 1, j], r.ry.at[a, d - 1, j], lane[j])
-
-    def e3(a, d):
-        for j in range(2):
-            third[a, d, j].wait_recv()
-        block = r.land.at[a, d, c]
-        fourth[a, d] = send(block, block, r.sm.at[a, d], r.rm.at[a, d], mate)
 
     def e4(a, d):
         fourth[a, d].wait_recv()
@@ -410,9 +412,12 @@
             r.hop[d, j] = value.astype(b16)
             hop[d, j] = send(r.hop.at[d, j], r.hop_in.at[d, j], r.sg.at[d, j], r.rg.at[d, j], lane[1 - j])
 
+    def direct(d):
+        return (2, 0, 1) if d >= 3 else (0, 1)
+
     def spread_start(d):
         block = r.home.at[d, :, mine]
-        for j in range(2):
+        for j in direct(d):
             spread[d, j] = send(block, block, r.sd.at[d, j], r.rd.at[d, j], lane[j])
 
     def reduce_end(d):
@@ -448,10 +453,12 @@
         for e in range(1, GROUPS):
             piece[d, e].wait_recv()
         block = r.op.at[:, d, :, mine_sub]
-        for j in range(2):
+        for j in direct(d):
             fan[d, j] = send(block, block, r.sq.at[d, j], r.rq.at[d, j], lane[j])
 
     def pass_start(d):
+        if len(direct(d)) == 3:
+            return
         for j in range(2):
             fan[d, j].wait_recv()
         for j in range(2):
@@ -459,6 +466,10 @@
             pass_on[d, j] = send(block, block, r.so.at[d, j], r.ro.at[d, j], lane[j])
 
     def pass_end(d):
+        if len(direct(d)) == 3:
+            for j in range(3):
+                fan[d, j].wait_recv()
+            return
         for j in range(2):
             pass_on[d, j].wait_recv()
 
@@ -467,6 +478,8 @@
         spread_start(d)
 
     def relay_start(d):
+        if len(direct(d)) == 3:
+            return
         for j in range(2):
             spread[d, j].wait_recv()
         for j in range(2):
@@ -474,6 +487,10 @@
             relay[d, j] = send(block, block, r.se.at[d, j], r.re.at[d, j], lane[j])
 
     def relay_end(d):
+        if len(direct(d)) == 3:
+            for j in range(3):
+                spread[d, j].wait_recv()
+            return
         for j in range(2):
             relay[d, j].wait_recv()
 
@@ -559,96 +576,96 @@
     loads["w_gate"].wait()
     loads["w_up"].wait()
     loads["w_down"].wait()
-    turn(1, 6, 2)
+    turn(2, 0, 2)
     e4(0, 0)
     e4(1, 0)
     forward(0)
     e1(*steps[0])
+    conv_forward()
     e1(*steps[1])
+    backward(0)
     turn(1, 2, 2)
     e1(*steps[2])
-    backward(0)
+    turn(0, 4, 2)
     e1(*steps[3])
+    turn(1, 0, 2)
+    turn(0, 2, 2)
+    e2(*steps[1])
+    e2(*steps[0])
+    turn(2, 4, 2)
     turn(1, 4, 2)
+    e2(*steps[2])
+    e1(*steps[5])
+    act_start()
+    turn(1, 6, 2)
+    e2(*steps[3])
+    e1(*steps[4])
+    reduce_start(0)
+    e3(*steps[1])
+    turn(0, 6, 2)
+    e3(*steps[0])
+    turn(2, 2, 2)
     turn(0, 0, 2)
-    conv_forward()
-    e2(*steps[0])
-    turn(2, 2, 2)
-    e2(*steps[1])
+    e3(*steps[2])
     turn(2, 6, 2)
-    e1(*steps[4])
-    turn(0, 2, 2)
-    e2(*steps[2])
-    e2(*steps[3])
-    e1(*steps[5])
-    turn(0, 6, 2)
-    turn(0, 4, 2)
-    act_start()
-    turn(1, 0, 2)
-    turn(2, 4, 2)
-    e3(*steps[1])
-    e3(*steps[0])
-    reduce_start(0)
-    e3(*steps[2])
-    e2(*steps[4])
-    turn(2, 0, 2)
-    e3(*steps[3])
     e4(0, 1)
     e4(1, 1)
     forward(1)
+    e3(*steps[3])
     e2(*steps[5])
     backward(1)
+    e2(*steps[4])
     reduce_mid(0)
     e4(0, 2)
     e4(1, 2)
     forward(2)
+    backward(2)
+    e3(*steps[5])
+    reduce_start(1)
     e3(*steps[4])
-    backward(2)
-    reduce_start(1)
-    e3(*steps[5])
     reduce_start(2)
     reduce_end(0)
     e4(0, 3)
     e4(1, 3)
     forward(3)
+    reduce_mid(1)
     backward(3)
-    reduce_mid(1)
-    weight_grad(0, 2)
     reduce_mid(2)
+    weight_grad(0, 3)
     reduce_start(3)
+    fan_start(0)
+    relay_start(0)
     reduce_end(1)
-    fan_start(0)
+    weight_grad(1, 0)
+    weight_grad(0, 0)
     reduce_end(2)
+    weight_grad(1, 1)
     reduce_mid(3)
-    relay_start(0)
     home_in(1)
+    pass_start(0)
+    weight_grad(2, 2)
+    weight_grad(2, 1)
     fan_start(1)
     reduce_end(3)
+    home_in(2)
+    fan_start(2)
+    pass_start(1)
+    relay_start(1)
+    relay_start(2)
+    home_in(3)
+    weight_grad(1, 2)
+    weight_grad(2, 0)
     weight_grad(2, 3)
-    weight_grad(2, 0)
-    pass_start(0)
-    weight_grad(1, 0)
-    home_in(2)
-    relay_start(1)
-    weight_grad(1, 2)
+    fan_start(3)
+    pass_start(2)
+    weight_grad(0, 2)
+    pass_start(3)
+    weight_grad(1, 3)
+    relay_start(3)
     weight_grad(0, 1)
-    pass_start(1)
-    fan_start(2)
-    weight_grad(0, 3)
-    home_in(3)
-    fan_start(3)
-    weight_grad(1, 1)
-    relay_start(2)
-    weight_grad(0, 0)
-    weight_grad(1, 3)
-    weight_grad(2, 2)
-    pass_start(2)
-    relay_start(3)
-    weight_grad(2, 1)
-    pass_start(3)
     rim_start()
+    stream_all()
     project()
-    stream_all()
     act_grad = last_dims(r.stream[...], r.v_out_proj[...])
     conv_grad = act_grad * r.v_gate_b[...].astype(f32)
     r.moe_in_grad[...] = r.full[:, mine]
@@ -715,7 +732,7 @@
         gate_c_grad=((tokens, chan), b16),
         value_x_grad=((tokens, chan), b16),
     )
-    loaded = [key for key in inputs if key not in ("routing", "route_weight")]
+    loaded = list(inputs)
     scratch = {"v_" + key: pltpu.VMEM(inputs[key].shape, inputs[key].dtype) for key in loaded}
     three, pair = GROUPS - 1, CORES * cap
     scratch |= dict(
@@ -765,10 +782,10 @@
         b=(GROUPS, 2, 2),
         g=(GROUPS, 2),
         c=(three,),
-        d=(GROUPS, 2),
+        d=(GROUPS, 3),
         e=(GROUPS, 2),
         p=(GROUPS, three),
-        q=(GROUPS, 2),
+        q=(GROUPS, 3),
         o=(GROUPS, 2),
         u=(three,),
         n=(1,),
@@ -780,7 +797,7 @@
     out = pl.pallas_call(
         functools.partial(step_kernel, names),
         out_shape=tuple(pltpu.VMEM(*shape) for shape in outputs.values()),
-        in_specs=[hbm if key in loaded else vmem for key in inputs],
+        in_specs=[hbm] * len(inputs),
         out_specs=(vmem,) * len(outputs),
         scratch_shapes=list(scratch.values()),
         compiler_params=pltpu.CompilerParams(

time: 57.5 us -> 55.1 us (0.958); the launches traced: 57.3 us -> 54.2 us
  Pallas kernels: 56.5 us -> 53.3 us
    pallas_call x1, Pallas kernels: 53.5 us -> 50.4 us  [on_device_paired(): pl.pallas_call(functools.partial(step_kernel, names), out_shape=tuple((pl...]
where the time goes in v3:
time: 55.1 us; the launch traced here: 54.2 us
  Pallas kernels  53.3 us (97%)
  between operations  0.81 us (1%)
    pallas_call x1, Pallas kernels, on_device_paired(): pl.pallas_call(functools.partial(step_kernel, names), out_shape=tuple((pl...  50.4 us
    pallas_call x1, Pallas kernels, on_device_paired(): pl.pallas_call(store_kernel, out_shape=tuple((jax.ShapeDtypeStruct(*shape...  2.92 us

profile of v3, /device:TPU:0, one launch (start us, length us, event | category | flops | bytes accessed | tf_op | source)
XLA Modules:
  0.0 54.2 jit_solution(11127516846788470431)
XLA Ops:
  0.6 50.4 %step.1 = (bf16[512,2048]{1,0:T(8,128)(2,1)S(1)}, bf16[512,2048]{1,0:T(8,128)(2,1)S(1)}, bf16[512,2048]{1,0:T(8,128)(2,1)S(1)}, bf16[192,512]{1,0:T(8,128)(2,1)S...) custom-call(s32[2,192]{1,0:T(2,128)} %bitcast.20, ...), custom_call_target="tpu_custom_call" | custom-call | tf_op jit(solution)/shard_map/step/pallas_call | solution.py:797
  51.1 2.9 %store.1 = (bf16[512,2048]{1,0:T(8,128)(2,1)}, bf16[512,2048]{1,0:T(8,128)(2,1)}, bf16[512,2048]{1,0:T(8,128)(2,1)}, bf16[192,512]{1,0:T(8,128)(2,1)}, f32[256,2...) custom-call(bf16[512,2048]{1,0:T(8,128)(2,1)S(1)} %get-tuple-element.24.refs_0_, ...), custom_call_target="tpu_custom_call" | custom-call | tf_op jit(solution)/shard_map/store/pallas_call | solution.py:808

commit v4 on v3

--- a/solution.py
+++ b/solution.py
@@ -199,7 +199,7 @@
     hid_rows = r.w_gate.shape[0]
     devices = CORES * GROUPS
     f32, b16 = jnp.float32, jnp.bfloat16
-    far = [z, z + 1 - 2 * lax.rem(z, 2), z + 2 - 4 * lax.div(z, 2), 3 - z]
+    far = [z, z + 1 - 2 * lax.rem(z, 2), 3 - z, z + 2 - 4 * lax.div(z, 2)]
     peer = [(CORES * far[d] + c, t) for d in range(GROUPS)]
     mate = (CORES * z + 1 - c, t)
     after, before = (lax.rem(s + 1, devices), t), (lax.rem(s + devices - 1, devices), t)
@@ -232,7 +232,8 @@
     group = lax.div(lead, CORES)
     low, high = lax.rem(group, 2), lax.div(group, 2)
     z_low, z_high = lax.rem(z, 2), lax.div(z, 2)
-    slot = (low + z_low - 2 * low * z_low) + 2 * (high + z_high - 2 * high * z_high)
+    odd, upper = low + z_low - 2 * low * z_low, high + z_high - 2 * high * z_high
+    slot = (odd + upper - 2 * odd * upper) + 2 * upper
     slot = slot.astype(f32)
     earlier = (column(slot) == slot) & (down < along)
     rank = jnp.sum(jnp.where(earlier, 1.0, 0.0), axis=0, keepdims=True)

time: 55.1 us -> 54.5 us (0.989)
  no operation moved by 1% of the time
where the time goes in v4:
time: 54.5 us; the launch traced here: 53.9 us
  Pallas kernels  53.1 us (97%)
  between operations  0.81 us (1%)
    pallas_call x1, Pallas kernels, on_device_paired(): pl.pallas_call(functools.partial(step_kernel, names), out_shape=tuple((pl...  50.2 us
    pallas_call x1, Pallas kernels, on_device_paired(): pl.pallas_call(store_kernel, out_shape=tuple((jax.ShapeDtypeStruct(*shape...  2.92 us

profile of v4, /device:TPU:0, one launch (start us, length us, event | category | flops | bytes accessed | tf_op | source)
XLA Modules:
  0.0 53.9 jit_solution(2708659855064825140)
XLA Ops:
  0.6 50.2 %step.1 = (bf16[512,2048]{1,0:T(8,128)(2,1)S(1)}, bf16[512,2048]{1,0:T(8,128)(2,1)S(1)}, bf16[512,2048]{1,0:T(8,128)(2,1)S(1)}, bf16[192,512]{1,0:T(8,128)(2,1)S...) custom-call(s32[2,192]{1,0:T(2,128)} %bitcast.20, ...), custom_call_target="tpu_custom_call" | custom-call | tf_op jit(solution)/shard_map/step/pallas_call | solution.py:798
  50.8 2.9 %store.1 = (bf16[512,2048]{1,0:T(8,128)(2,1)}, bf16[512,2048]{1,0:T(8,128)(2,1)}, bf16[512,2048]{1,0:T(8,128)(2,1)}, bf16[192,512]{1,0:T(8,128)(2,1)}, f32[256,2...) custom-call(bf16[512,2048]{1,0:T(8,128)(2,1)S(1)} %get-tuple-element.24.refs_0_, ...), custom_call_target="tpu_custom_call" | custom-call | tf_op jit(solution)/shard_map/store/pallas_call | solution.py:809
